TPU v7x, 512 devices: a whole 4x4x16 slice. The times are simulated.
512 devices in a mesh: sp: 128 (over z, x, core), tp: 4 (over y).
Axes of the slice: x: 4, y: 4, z: 16, core: 2. Of those that a mesh axis runs over, the one named last changes fastest.
Arguments:
- tokens: bfloat16 [65536, 2048], P(('sp', 'tp')), may hold values from -8 to 8
- in_gain: float32 [2048], replicated, may hold values from 0.1 to 1.9
- w_conv_val: bfloat16 [2048, 1024], P('sp', 'tp'), may hold values from -0.125 to 0.125
- w_conv_gate: bfloat16 [2048, 1024], P('sp', 'tp'), may hold values from -0.125 to 0.125
- w_query: bfloat16 [2048, 1024], P('sp', 'tp'), may hold values from -1 to 1
- w_key: bfloat16 [2048, 256], P('sp', 'tp'), may hold values from -1 to 1
- value_weight: bfloat16 [2048, 256], P('sp', 'tp'), may hold values from -0.125 to 0.125
- conv_taps: float32 [31, 1024], P(None, 'tp'), may hold values from -1 to 1
- conv_bias: float32 [1024], P('tp'), may hold values from -3 to 3
- norm_gain: float32 [1024], P('tp'), may hold values from 0.1 to 1.9
- norm_bias: float32 [1024], P('tp'), may hold values from -3 to 3
- head_sink_logit: float32 [16], P('tp'), may hold values from 4 to 7
- w_out_conv: bfloat16 [1024, 2048], P('tp', 'sp'), may hold values from -0.125 to 0.125
- w_out_attn: bfloat16 [1024, 2048], P('tp', 'sp'), may hold values from -0.125 to 0.125
Outputs:
- mixed: bfloat16 [65536, 2048], P(('sp', 'tp'))
- log_total: float32 [65536, 16], P('sp', 'tp')
All inputs are finite; a program needn't handle non-finite values.
Results may differ from a plain program's by a relative error of at most 0.012.
Values may be sent and summed in bfloat16 or wider, within the bound.
A program may use at most 64 MiB of HBM per device.

v0:
```python
import jax
import jax.numpy as jnp
from jax import lax
from jax.sharding import Mesh
from jax.sharding import PartitionSpec as P

WINDOW_REACH = 128
SP = ("sp_0", "sp_1", "sp_2")
SP_TP = ("sp_0", "sp_1", "sp_2", "tp")


def sent_together(arrays, axis, dim, along):
    widths = [a.shape[along] for a in arrays]
    both = jnp.concatenate(arrays, axis=along)
    filled = lax.all_gather(both, axis, axis=dim, tiled=True)
    return tuple(jnp.split(filled, [sum(widths[:k]) for k in range(1, len(widths))], axis=along))


def from_everyone(array, axis):
    copies = jnp.broadcast_to(array, (lax.axis_size(axis), *array.shape))
    return lax.all_to_all(copies, axis, split_axis=0, concat_axis=0, tiled=True)


def in_order(blocks, dim):
    blocks = jnp.moveaxis(blocks, 0, dim)
    shape = blocks.shape
    return blocks.reshape(*shape[:dim], shape[dim] * shape[dim + 1], *shape[dim + 2 :])


def gather_directly(array, axis, dim):
    blocks = from_everyone(array, axis)
    return in_order(blocks, dim)


def with_halo(cells, sides, width):
    for axis, dim in sides:
        count = lax.axis_size(axis)
        ends = count - 1
        head = lax.slice_in_dim(cells, 0, width, axis=dim)
        tail = lax.slice_in_dim(cells, cells.shape[dim] - width, cells.shape[dim], axis=dim)
        cells = jnp.concatenate(
            [
                lax.ppermute(tail, axis, [(i, (i + 1) % count) for i in range(ends)]),
                cells,
                lax.ppermute(head, axis, [((i + 1) % count, i) for i in range(ends)]),
            ],
            axis=dim,
        )
    return cells


def over_copies(array, axis):
    everything = from_everyone(array, axis)
    return jnp.sum(everything, axis=0)


def in_one(arrays, axis):
    vector, at, outs = (jnp.concatenate([a.reshape(-1) for a in arrays]), 0, [])
    running = over_copies(vector, axis)
    for a in arrays:
        outs.append(running[at : at + a.size].reshape(a.shape))
        at += a.size
    return tuple(outs)


def whole_of(array, axes, dim):
    far, near = axes
    initial = from_everyone(array, far)
    blocks = jnp.swapaxes(from_everyone(initial, near), 0, 1)
    return in_order(blocks.reshape(-1, *array.shape), dim)


def side_by_side(arrays, axis, dim, along):
    widths = [a.shape[along] for a in arrays]
    both = jnp.concatenate(arrays, axis=along)
    filled = whole_of(both, axis, dim)
    return tuple(jnp.split(filled, [sum(widths[:k]) for k in range(1, len(widths))], axis=along))


def cut_along(array, dim, peers):
    before, after = (array.shape[:dim], array.shape[dim + 1 :])
    return jnp.moveaxis(array.reshape(*before, peers, -1, *after), dim, 0)


def sent_and_summed(array, axis, dim):
    blocks = cut_along(array, dim, lax.axis_size(axis))
    arrived = lax.all_to_all(blocks, axis, split_axis=0, concat_axis=0, tiled=True)
    return arrived.astype(jnp.float32).sum(axis=0)


def on_device(
    tokens,
    in_gain,
    w_conv_val,
    w_conv_gate,
    w_query,
    w_key,
    value_weight,
    conv_taps,
    conv_bias,
    norm_gain,
    norm_bias,
    head_sink_logit,
    w_out_conv,
    w_out_attn,
):
    flt = tokens.astype(jnp.float32)
    normed = (
        flt * lax.rsqrt(jnp.mean(flt * flt, axis=-1, keepdims=True) + 1e-06) * in_gain
    ).astype(jnp.bfloat16)
    val_full, gate_full, query_full, key_full, value_full = sent_together(
        (w_conv_val, w_conv_gate, w_query, w_key, value_weight), SP, 0, 1
    )
    joined = jnp.concatenate([val_full, gate_full, query_full, key_full, value_full], axis=1)
    projected = jnp.dot(
        gather_directly(normed, "tp", 0), joined, preferred_element_type=jnp.float32
    )
    chans = val_full.shape[1]
    qwidth = query_full.shape[1]
    kwidth = key_full.shape[1]
    length = projected.shape[0]
    glu = (projected[:, :chans] * jax.nn.sigmoid(projected[:, chans : 2 * chans])).astype(
        jnp.bfloat16
    )
    base = 2 * chans
    query_matrix = projected[:, base : base + qwidth].astype(jnp.bfloat16)
    key = projected[:, base + qwidth : base + qwidth + kwidth].astype(jnp.bfloat16)
    value_matrix = projected[:, base + qwidth + kwidth :].astype(jnp.bfloat16)
    taps = conv_taps.shape[0]
    half = taps // 2
    padded = with_halo(glu, ((SP, 0),), half)
    filtered = jnp.zeros(glu.shape, jnp.float32) + conv_bias
    for offset in range(taps):
        filtered = (
            filtered + padded[offset : offset + length].astype(jnp.float32) * conv_taps[offset]
        )
    sums, squares = in_one(
        (jnp.sum(filtered, axis=-1), jnp.sum(filtered * filtered, axis=-1)), "tp"
    )
    count = chans * lax.axis_size("tp")
    center = (sums / count)[:, None]
    spread = (squares / count)[:, None] - center * center
    conv_out = jax.nn.silu(
        (filtered - center) * lax.rsqrt(spread + 1e-05) * norm_gain + norm_bias
    ).astype(jnp.bfloat16)
    heads_here = head_sink_logit.shape[0]
    head_size = qwidth // heads_here
    kv_here = kwidth // head_size
    query_groups = heads_here // kv_here
    stacked = jnp.stack([key, value_matrix], axis=0)
    banded = with_halo(stacked, ((SP, 1),), WINDOW_REACH)
    span = length + 2 * WINDOW_REACH
    key_band = banded[0].reshape(span, kv_here, head_size)
    value_band = banded[1].reshape(span, kv_here, head_size)
    query4_grouped = query_matrix.reshape(length, kv_here, query_groups, head_size)
    scores = jnp.einsum(
        "qkgd,jkd->kgqj", query4_grouped, key_band, preferred_element_type=jnp.float32
    ) * head_size ** (-0.5)
    offset_pos = lax.axis_index(SP) * length
    seq_len = length * lax.axis_size(SP)
    qpos = offset_pos + jnp.arange(length, dtype=jnp.int32)
    kpos = offset_pos - WINDOW_REACH + jnp.arange(span, dtype=jnp.int32)
    valid = (
        (jnp.abs(qpos[:, None] - kpos[None, :]) <= WINDOW_REACH)
        & (kpos[None, :] >= 0)
        & (kpos[None, :] < seq_len)
    )
    sink_column = head_sink_logit.reshape(kv_here, query_groups, 1)
    masked = jnp.where(valid, scores, -1e30)
    top = jnp.maximum(jnp.max(masked, axis=-1), sink_column)
    expd = jnp.where(valid, jnp.exp(masked - top[..., None]), 0.0)
    total = jnp.sum(expd, axis=-1) + jnp.exp(sink_column - top)
    probs = (expd / total[..., None]).astype(jnp.bfloat16)
    attended = jnp.einsum(
        "kgqj,jkd->qkgd", probs, value_band, preferred_element_type=jnp.float32
    ).astype(jnp.bfloat16)
    attended = attended.reshape(length, qwidth)
    log_total = (top + jnp.log(total)).reshape(heads_here, length).T
    out_conv_cols, out_attn_cols = side_by_side(
        (w_out_conv, w_out_attn), (("sp_0", "sp_1"), "sp_2"), 1, 0
    )
    out_rows = jnp.concatenate([out_conv_cols, out_attn_cols], axis=0)
    features = jnp.concatenate([conv_out, attended], axis=1)
    mixed = sent_and_summed(
        jnp.dot(features, out_rows, preferred_element_type=jnp.float32).astype(jnp.bfloat16),
        "tp",
        0,
    ).astype(jnp.bfloat16)
    return (mixed, log_total)


def solution(mesh):
    finer = Mesh(mesh.devices.reshape(16, 4, 2, mesh.shape["tp"]), ("sp_0", "sp_1", "sp_2", "tp"))
    in_specs = (
        P(SP_TP, None),
        P(),
        P(SP, "tp"),
        P(SP, "tp"),
        P(SP, "tp"),
        P(SP, "tp"),
        P(SP, "tp"),
        P(None, "tp"),
        P("tp"),
        P("tp"),
        P("tp"),
        P("tp"),
        P("tp", SP),
        P("tp", SP),
    )
    out_specs = (P(SP_TP, None), P(SP, "tp"))
    return jax.shard_map(
        on_device, mesh=finer, in_specs=in_specs, out_specs=out_specs, check_vma=False
    )
```

profile of v0, /device:TPU:1, one launch (start us, length us, event | category | flops | bytes accessed | tf_op | source)
XLA Modules:
  0.0 237.2 jit_solution(10012362763361222723)
XLA Ops:
  7.2 0.0 all-gather.2.cloned.1.call-start
  7.2 1.4 concatenate.55
  8.7 0.0 all-gather.2.cloned.1.call-update
  8.7 0.7 pad_maximum_fusion.5
  9.4 1.1 broadcast_in_dim.42
  10.5 19.1 %all-to-all-start.2 = ((bf16[64,512,16]{1,2,0:T(8,128)(2,1)}), bf16[64,512,16]{1,2,0:T(8,128)(2,1)S(1)}, u32[]{:S(2)}, u32[]{:S(2)}) async-start(bf16[64,512,16]{1,2,0:T(8,128)(2,1)} %broadcast_in_dim.42), calls=%async_computation.2 | async-start | bytes 2097152 | tf_op jit(solution)/shard_map/all_to_all | solution.py:21
  29.6 1.2 fusion.12
  30.9 1.2 fusion.14
  32.1 51.1 %all-to-all-done.2 = bf16[64,512,16]{1,2,0:T(8,128)(2,1)S(1)} async-done(((bf16[64,512,16]{1,2,0:T(8,128)(2,1)}), bf16[64,512,16]{1,2,0:T(8,128)(2,1)S(1)}, u32[]{:S(2)}, u32[]{:S(2)}) %all-to-all-start.2) | async-done | bytes 1048608 | tf_op jit(solution)/shard_map/all_to_all | solution.py:21
  83.2 0.3 broadcast_in_dim.43
  83.5 9.7 %all_to_all.26 = bf16[2,64,512,16]{2,3,1,0:T(8,128)(2,1)S(1)} all-to-all(bf16[2,64,512,16]{2,3,1,0:T(8,128)(2,1)S(1)} %broadcast_in_dim.43), channel_id=1, replica_groups=mesh['sp_0'=16,'sp_1'=4,'sp_2'=2,'tp'=4] {'sp_2'}, dimensions={0} | all-to-all | bytes 4194304 | tf_op jit(solution)/shard_map/all_to_all | solution.py:21
  93.2 1.6 broadcast_in_dim.20
  94.8 4.4 %all-to-all-start = ((bf16[4,128,2048]{2,1,0:T(8,128)(2,1)}), bf16[4,128,2048]{2,1,0:T(8,128)(2,1)}, u32[]{:S(2)}, u32[]{:S(2)}) async-start(bf16[4,128,2048]{2,1,0:T(8,128)(2,1)} %broadcast_in_dim.20), calls=%async_computation | async-start | bytes 4194304 | tf_op jit(solution)/shard_map/all_to_all | solution.py:21
  99.4 0.8 fusion.8
  100.2 0.2 copy.45
  100.4 1.2 fusion.62
  101.6 23.7 %all-to-all-done = bf16[4,128,2048]{2,1,0:T(8,128)(2,1)} async-done(((bf16[4,128,2048]{2,1,0:T(8,128)(2,1)}), bf16[4,128,2048]{2,1,0:T(8,128)(2,1)}, u32[]{:S(2)}, u32[]{:S(2)}) %all-to-all-start) | async-done | bytes 2097184 | tf_op jit(solution)/shard_map/all_to_all | solution.py:21
  125.3 38.2 %all-gather.2.cloned.1.call-done = bf16[2048,896]{1,0:T(8,128)(2,1)} async-done(((bf16[16,896]{1,0:T(8,128)(2,1)}), bf16[2048,896]{1,0:T(8,128)(2,1)}) %all-gather.2.cloned.1.call-update) | async-done | bytes 3670032 | tf_op jit(solution)/shard_map/all_gather | solution.py:15
  163.5 5.0 %fusion.66 = (bf16[512,896]{1,0:T(8,128)(2,1)S(1)}, f32[512,896]{1,0:T(8,128)S(1)}) fusion(bf16[512,2048]{1,0:T(8,128)(2,1)} %bitcast, bf16[2048,896]{1,0:T(8,128)(2,1)} %all-gather.2.cloned.1.call-done), kind=kOutput, calls=%fused_computation.139 | convolution fusion | flops 1879506944 | bytes 8519680 | tf_op jit(solution)/shard_map/dot_general | solution.py:115
  168.5 0.0 copy-start.5
  168.6 0.0 copy-start.6
  168.6 0.1 fusion.22
  168.7 2.0 collective-permute-start
  170.7 2.4 collective-permute-start.1
  173.1 0.1 slice_bitcast_fusion.5
  173.2 2.5 %collective-permute-done.1 = bf16[15,256]{1,0:T(8,128)(2,1)S(1)} collective-permute-done((bf16[15,256]{1,0:T(8,128)(2,1)S(1)}, bf16[15,256]{1,0:T(8,128)(2,1)S(1)}, u32[]{:S(2)}, u32[]{:S(2)}) %collective-permute-start.1) | collective-permute-done | bytes 7712 | tf_op jit(solution)/shard_map/ppermute | solution.py:45
  175.7 2.7 %fusion.61 = (f32[512]{0:T(512)S(1)}, f32[512]{0:T(512)S(1)}, f32[512,256]{1,0:T(8,128)S(1)}) fusion(f32[256]{0:T(256)S(1)} %bitcast.116, bf16[15,256]{1,0:T(8,128)(2,1)S(1)} %collective-permute-done.1, bf16[512,256]{1,0:T(8,128)(2,1)S(1)} %fusion.22, f32[256]{0:T(256)S(1)} %bitcast.117, f32[256]{0:T(256)S(1)} %bitcast.119, f32[256]{0:T(256)S(1)} %bitcast.120, ...), kind=kLoop, calls=%fused_computation.134 | loop fusion | flops 24378368 | bytes 838656 | tf_op jit(solution)/shard_map/reduce_sum | solution.py:138
  178.4 0.6 broadcast_in_dim.38
  179.0 3.9 %all-to-all-start.1 = ((f32[4,1,1024]{2,1,0:T(1,128)}), f32[4,1,1024]{2,1,0:T(1,128)S(1)}, u32[]{:S(2)}, u32[]{:S(2)}) async-start(f32[4,1,1024]{2,1,0:T(1,128)} %broadcast_in_dim.38), calls=%async_computation.1 | async-start | bytes 32768 | tf_op jit(solution)/shard_map/all_to_all | solution.py:21
  182.9 1.0 slice.396
  183.9 2.2 collective-permute-start.2
  186.1 2.3 collective-permute-start.3
  188.4 0.1 copy.40
  188.7 0.0 copy-start.3
  188.7 0.3 multiply_convert_fusion
  188.9 2.8 %collective-permute-done.3 = bf16[2,128,64]{2,1,0:T(8,128)(2,1)S(1)} collective-permute-done((bf16[2,128,64]{2,1,0:T(8,128)(2,1)S(1)}, bf16[2,128,64]{2,1,0:T(8,128)(2,1)S(1)}, u32[]{:S(2)}, u32[]{:S(2)}) %collective-permute-start.3) | collective-permute-done | bytes 32800 | tf_op jit(solution)/shard_map/ppermute | solution.py:45
  191.7 0.1 pad_maximum_fusion
  191.8 1.1 fusion
  193.0 0.1 broadcast_maximum_fusion
  193.1 1.6 fusion.1
  194.6 0.1 exponential_add_fusion
  194.7 2.2 fusion.9
  196.9 0.1 copy.44
  197.0 2.6 %convolution_convert_fusion = bf16[512,2048]{1,0:T(8,128)(2,1)} fusion(bf16[256,2048]{0,1:T(8,128)(2,1)S(1)} %bitcast.104, bf16[256,2048]{0,1:T(8,128)(2,1)S(1)} %bitcast.103, bf16[512,256]{1,0:T(8,128)(2,1)S(1)} %copy.44, bf16[512,256]{1,0:T(8,128)(2,1)S(1)} %multiply_convert_fusion), kind=kOutput, calls=%fused_computation.7 | convolution fusion | flops 1080033280 | bytes 4718592 | tf_op jit(solution)/shard_map/dot_general | solution.py:185
  199.7 4.5 %all-to-all-start.4 = ((bf16[4,128,2048]{2,1,0:T(8,128)(2,1)}), bf16[4,128,2048]{2,1,0:T(8,128)(2,1)S(1)}, u32[]{:S(2)}, u32[]{:S(2)}) async-start(bf16[4,128,2048]{2,1,0:T(8,128)(2,1)} %bitcast.101), calls=%async_computation.4 | async-start | bytes 4194304 | tf_op jit(solution)/shard_map/all_to_all | solution.py:87
  204.2 0.7 fusion.53
  204.9 24.2 %all-to-all-done.4 = bf16[4,128,2048]{2,1,0:T(8,128)(2,1)S(1)} async-done(((bf16[4,128,2048]{2,1,0:T(8,128)(2,1)}), bf16[4,128,2048]{2,1,0:T(8,128)(2,1)S(1)}, u32[]{:S(2)}, u32[]{:S(2)}) %all-to-all-start.4) | async-done | bytes 2097184 | tf_op jit(solution)/shard_map/all_to_all | solution.py:87
  229.1 1.3 reduce_sum.64
  (25 shorter events, 0.2 us)
Async XLA Ops:
  7.2 156.4 %all-gather.2.cloned.1.call-start = ((), (), s32[]{:S(2)}) async-start(), calls=%async_computation.5 | async-start | bytes 3698688 | tf_op jit(solution)/shard_map/all_gather | solution.py:15
  10.5 72.7 %all-to-all-start.2 = ((bf16[64,512,16]{1,2,0:T(8,128)(2,1)}), bf16[64,512,16]{1,2,0:T(8,128)(2,1)S(1)}, u32[]{:S(2)}, u32[]{:S(2)}) async-start(bf16[64,512,16]{1,2,0:T(8,128)(2,1)} %broadcast_in_dim.42), calls=%async_computation.2 | async-start | bytes 2097152 | tf_op jit(solution)/shard_map/all_to_all | solution.py:21
  93.2 6.1 %copy-start.2 = (f32[31,256]{1,0:T(8,128)S(1)}, f32[31,256]{1,0:T(8,128)}, u32[]{:S(2)}) copy-start(f32[31,256]{1,0:T(8,128)} %param.21) | copy-start | bytes 95236
  94.8 30.5 %all-to-all-start = ((bf16[4,128,2048]{2,1,0:T(8,128)(2,1)}), bf16[4,128,2048]{2,1,0:T(8,128)(2,1)}, u32[]{:S(2)}, u32[]{:S(2)}) async-start(bf16[4,128,2048]{2,1,0:T(8,128)(2,1)} %broadcast_in_dim.20), calls=%async_computation | async-start | bytes 4194304 | tf_op jit(solution)/shard_map/all_to_all | solution.py:21
  163.5 12.2 %copy-start.4 = (f32[256]{0:T(256)S(1)}, f32[256]{0:T(256)}, u32[]{:S(2)}) copy-start(f32[256]{0:T(256)} %param.22) | copy-start | bytes 3076
  168.5 7.2 %copy-start.1 = (bf16[512,896]{1,0:T(8,128)(2,1)}, bf16[512,896]{1,0:T(8,128)(2,1)S(1)}, u32[]{:S(2)}) copy-start(bf16[512,896]{1,0:T(8,128)(2,1)S(1)} %get-tuple-element.46) | copy-start | bytes 2752516
  168.5 20.1 %copy-start.5 = (f32[256]{0:T(256)S(1)}, f32[256]{0:T(256)}, u32[]{:S(2)}) copy-start(f32[256]{0:T(256)} %param.24) | copy-start | bytes 3076
  168.6 20.1 %copy-start.6 = (f32[256]{0:T(256)S(1)}, f32[256]{0:T(256)}, u32[]{:S(2)}) copy-start(f32[256]{0:T(256)} %param.23) | copy-start | bytes 3076
  168.7 4.5 %collective-permute-start = (bf16[15,256]{1,0:T(8,128)(2,1)S(1)}, bf16[15,256]{1,0:T(8,128)(2,1)S(1)}, u32[]{:S(2)}, u32[]{:S(2)}) collective-permute-start(bf16[15,256]{1,0:T(8,128)(2,1)S(1)} %get-tuple-element.9), channel_id=1, source_target_pairs={{0,4},{4,8},{8,12},{12,16},{16,20},{20,24},{24,28},{28,32},{32,36}... | collective-permute-start | bytes 23048 | tf_op jit(solution)/shard_map/ppermute | solution.py:43
  170.7 5.0 %collective-permute-start.1 = (bf16[15,256]{1,0:T(8,128)(2,1)S(1)}, bf16[15,256]{1,0:T(8,128)(2,1)S(1)}, u32[]{:S(2)}, u32[]{:S(2)}) collective-permute-start(bf16[15,256]{1,0:T(8,128)(2,1)S(1)} %get-tuple-element.10), channel_id=1, source_target_pairs={{4,0},{8,4},{12,8},{16,12},{20,16},{24,20},{28,24},{32,28},{36,32}... | collective-permute-start | bytes 23048 | tf_op jit(solution)/shard_map/ppermute | solution.py:45
  179.0 9.6 %all-to-all-start.1 = ((f32[4,1,1024]{2,1,0:T(1,128)}), f32[4,1,1024]{2,1,0:T(1,128)S(1)}, u32[]{:S(2)}, u32[]{:S(2)}) async-start(f32[4,1,1024]{2,1,0:T(1,128)} %broadcast_in_dim.38), calls=%async_computation.1 | async-start | bytes 32768 | tf_op jit(solution)/shard_map/all_to_all | solution.py:21
  183.9 5.0 %collective-permute-start.2 = (bf16[2,128,64]{2,1,0:T(8,128)(2,1)S(1)}, bf16[2,128,64]{2,1,0:T(8,128)(2,1)S(1)}, u32[]{:S(2)}, u32[]{:S(2)}) collective-permute-start(bf16[2,128,64]{2,1,0:T(8,128)(2,1)S(1)} %get-tuple-element.11), channel_id=1, source_target_pairs={{0,4},{4,8},{8,12},{12,16},{16,20},{20,24},{24,28},{28,32},{32,36}... | collective-permute-start | bytes 98312 | tf_op jit(solution)/shard_map/ppermute | solution.py:43
  186.1 5.6 %collective-permute-start.3 = (bf16[2,128,64]{2,1,0:T(8,128)(2,1)S(1)}, bf16[2,128,64]{2,1,0:T(8,128)(2,1)S(1)}, u32[]{:S(2)}, u32[]{:S(2)}) collective-permute-start(bf16[2,128,64]{2,1,0:T(8,128)(2,1)S(1)} %get-tuple-element.12), channel_id=1, source_target_pairs={{4,0},{8,4},{12,8},{16,12},{20,16},{24,20},{28,24},{32,28},{36,32}... | collective-permute-start | bytes 98312 | tf_op jit(solution)/shard_map/ppermute | solution.py:45
  188.7 4.3 %copy-start.3 = (f32[4]{0:T(128)S(1)}, f32[4]{0:T(128)}, u32[]{:S(2)}) copy-start(f32[4]{0:T(128)} %param.25) | copy-start | bytes 52
  194.7 2.3 copy-start
  199.7 29.4 %all-to-all-start.4 = ((bf16[4,128,2048]{2,1,0:T(8,128)(2,1)}), bf16[4,128,2048]{2,1,0:T(8,128)(2,1)S(1)}, u32[]{:S(2)}, u32[]{:S(2)}) async-start(bf16[4,128,2048]{2,1,0:T(8,128)(2,1)} %bitcast.101), calls=%async_computation.4 | async-start | bytes 4194304 | tf_op jit(solution)/shard_map/all_to_all | solution.py:87
Sparse Core Ops, SparseCore 0:
  11.6 151.8 all-gather.1
where the time goes:
time: 240 us; the launch traced here: 237 us
  waiting for transfers between devices  143 us (60%)
  starting transfers between devices  40.8 us (17%)
  between operations  14.3 us (6%)
  matrix products  11 us (5%)
  other arithmetic  10.9 us (5%)
  blocking collectives  9.68 us (4%)
  local copies, waits for them, and re-layouts  7.93 us (3%)
    all_to_all x3, waiting for transfers between devices, from_everyone(): return lax.all_to_all(copies, axis, split_axis=0, concat_axis=0, tiled=True)  74.8 us
    all_gather x1, waiting for transfers between devices, sent_together(): filled = lax.all_gather(both, axis, axis=dim, tiled=True)  38.2 us
    all_to_all x3, starting transfers between devices, from_everyone(): return lax.all_to_all(copies, axis, split_axis=0, concat_axis=0, tiled=True)  27.4 us
    all_to_all x1, waiting for transfers between devices, sent_and_summed(): lax.all_to_all(blocks, axis, split_axis=0, concat_axis=0, tiled=True)  24.2 us
    all_to_all x1, blocking collectives, from_everyone(): return lax.all_to_all(copies, axis, split_axis=0, concat_axis=0, tiled=True)  9.68 us
    ppermute x2, waiting for transfers between devices, with_halo(): lax.ppermute(head, axis, [((i + 1) % count, i) for i in range(ends)])  5.28 us
    dot_general x1, matrix products, on_device(): jnp.dot(gather_directly(normed, 'tp', 0), joined, preferred_element_type=...  5.01 us
  transfers between devices with their start and end apart: 9, of which 6 were waited for; matrix products, arithmetic and copies ran while one was open for 5% of the time, Pallas kernels for 0%

commit v1 on v0

v1 whole, which is shorter than its diff:
```python
import jax
import jax.numpy as jnp
from jax import lax
from jax.experimental import pallas as pl
from jax.experimental.pallas import tpu as pltpu
from jax.sharding import Mesh
from jax.sharding import PartitionSpec as P

MESH = pl.DeviceIdType.MESH
REACH = 128
HEADS = 4
HALF = 15
RING = 16
LAG_RELAY = 1
LAG_PAIR = 2
F32 = jnp.float32
BF16 = jnp.bfloat16
SP = ("z", "x", "c")
SP_TP = ("z", "x", "c", "y")


def nt_dot(a, b):
    return lax.dot_general(a, b, (((1,), (1,)), ((), ())), preferred_element_type=F32)


def layer(
    tok, gain, w_val, w_gate, w_q, w_k, w_v, w_oc, w_oa, taps, cbias, ngain, nbias, sink,
    mixed, log_out,
    wg, og, tg, glu_s, q_s, kv_s, kvw, padf, filt, stat, st_tx, st_rx, feat, mask_s,
    part, tx2, rx2, txp, rxp,
    r_wz, s_wz, r_wx, s_wx, r_wp, s_wp, r_ox, s_ox, r_oz, s_oz, r_op, s_op, r_t, s_t,
    r_h, s_h, r_st, s_st, r_r2, s_r2, r_rp, s_rp,
):
    z, x, c, y = (lax.axis_index(n) for n in ("z", "x", "c", "y"))
    d = 1 - 2 * c
    zp, zm = lax.rem(z + 1, 16), lax.rem(z + 15, 16)
    xr, xl = lax.rem(x + 4 + d, 4), lax.rem(x + 4 - d, 4)
    x2 = lax.rem(x + 2, 4)
    yp, ym, y2 = lax.rem(y + 1, 4), lax.rem(y + 3, 4), lax.rem(y + 2, 4)
    other = 1 - c
    me = z * 8 + x * 2 + c
    nxt, prv = lax.rem(me + 1, 128), lax.rem(me + 127, 128)

    def at_sp(s):
        return {"z": s // 8, "x": lax.rem(s // 2, 4), "c": lax.rem(s, 2)}

    def copy(src, dst, ssem, rsem, dev):
        return pltpu.make_async_remote_copy(
            src_ref=src, dst_ref=dst, send_sem=ssem, recv_sem=rsem,
            device_id=dev, device_id_type=MESH,
        )

    sent = []

    def send(src, dst, ssem, rsem, dev):
        cp = copy(src, dst, ssem, rsem, dev)
        cp.start()
        sent.append(cp)

    def got(dst, ssem, rsem, dev):
        copy(dst, dst, ssem, rsem, dev).wait_recv()

    barrier = pltpu.get_barrier_semaphore()
    greet = [{"z": zp}, {"z": zm}, {"x": xr}, {"x": xl}, {"c": other}, {"y": yp}, {"y": ym}, {"y": y2},
             at_sp(nxt), at_sp(prv)]
    for dev in greet:
        pl.semaphore_signal(barrier, inc=1, device_id=dev, device_id_type=MESH)

    wg[z, x, c] = jnp.concatenate([w_val[...], w_gate[...], w_q[...], w_k[...], w_v[...]], axis=1)
    eye = (
        lax.broadcasted_iota(jnp.int32, (16, 16), 0) == lax.broadcasted_iota(jnp.int32, (16, 16), 1)
    ).astype(BF16)
    og[z, x, c] = jnp.concatenate([nt_dot(eye, w_oc[...]), nt_dot(eye, w_oa[...])], axis=1).astype(BF16)
    t = tok[...].astype(F32)
    inv = lax.rsqrt(jnp.mean(t * t, axis=-1, keepdims=True) + 1e-06)
    normed = (t * inv * gain[...]).astype(BF16)
    tg[y, 0] = normed[:, :1024]
    tg[y, 1] = normed[:, 1024:]
    row = lax.broadcasted_iota(jnp.int32, (128, 384), 0)
    col = lax.broadcasted_iota(jnp.int32, (128, 384), 1)
    mask_s[...] = jnp.where((col >= row) & (col <= row + 2 * REACH), 0.0, -1e30).astype(F32)

    pl.semaphore_wait(barrier, len(greet))

    send(tg.at[y, 0], tg.at[y, 0], s_t.at[0], r_t.at[0], {"y": yp})
    send(tg.at[y, 1], tg.at[y, 1], s_t.at[1], r_t.at[1], {"y": ym})
    def wblk(zi, xi):
        return wg.at[zi, xi, c]

    def oblk(zi, h):
        return og.at[zi, 2 * h : 2 * h + 2, c]

    def plus(k):
        return lax.rem(z + 16 - k, 16)

    def minus(k):
        return lax.rem(z + k, 16)

    def w_forward(k, up):
        zi = plus(k) if up else minus(k)
        i = k if up else 8 + k
        send(wblk(zi, x), wblk(zi, x), s_wz.at[i], r_wz.at[i], {"z": zp if up else zm})

    def o_forward(k, up, h):
        zi = plus(k) if up else minus(k)
        i = 2 * (k if up else 8 + k) + h
        send(oblk(zi, h), oblk(zi, h), s_oz.at[i], r_oz.at[i], {"z": zp if up else zm})

    def w_sideways(zi, r):
        send(wblk(zi, x), wblk(zi, x), s_wx.at[r], r_wx.at[r], {"x": xr})
        send(wblk(zi, x), wblk(zi, x), s_wx.at[16 + r], r_wx.at[16 + r], {"x": xl})

    def members(k):
        out = []
        if 0 <= k <= 8:
            out.append((plus(k), k))
        if 1 <= k <= 7:
            out.append((minus(k), 8 + k))
        return out

    own_o = og.at[z, x, c]
    send(own_o, own_o, s_ox.at[0], r_ox.at[0], {"x": xr})
    send(own_o, own_o, s_ox.at[1], r_ox.at[1], {"x": xl})
    for k in range(0, 9 + LAG_PAIR):
        if k == 0:
            w_forward(0, True)
            w_forward(0, False)
        if 1 <= k <= 8:
            got(wblk(plus(k), x), s_wz.at[k - 1], r_wz.at[k - 1], {"z": zm})
            if k < 8:
                w_forward(k, True)
        if 1 <= k <= 7:
            got(wblk(minus(k), x), s_wz.at[8 + k - 1], r_wz.at[8 + k - 1], {"z": zp})
            if k < 7:
                w_forward(k, False)
        for zi, r in members(k):
            w_sideways(zi, r)
        if k == 0:
            send(tg.at[y, 1], tg.at[y, 1], s_t.at[2], r_t.at[2], {"y": yp})
            send(tg.at[y, 0], tg.at[y, 0], s_t.at[3], r_t.at[3], {"y": ym})
            from_l, from_r = og.at[z, xl, c], og.at[z, xr, c]
            got(from_l, s_ox.at[0], r_ox.at[0], {"x": xl})
            send(from_l, from_l, s_ox.at[2], r_ox.at[2], {"x": xr})
            got(from_r, s_ox.at[1], r_ox.at[1], {"x": xr})
            got(og.at[z, x2, c], s_ox.at[2], r_ox.at[2], {"x": xl})
            for h in range(2):
                o_forward(0, True, h)
                o_forward(0, False, h)
        for h in range(2):
            if 1 <= k <= 8:
                got(oblk(plus(k), h), s_oz.at[2 * (k - 1) + h], r_oz.at[2 * (k - 1) + h], {"z": zm})
                if k < 8:
                    o_forward(k, True, h)
            if 1 <= k <= 7:
                i = 2 * (8 + k - 1) + h
                got(oblk(minus(k), h), s_oz.at[i], r_oz.at[i], {"z": zp})
                if k < 7:
                    o_forward(k, False, h)
        for zi, r in members(k):
            send(og.at[zi, :, c], og.at[zi, :, c], s_op.at[r], r_op.at[r], {"c": other})
        for zi, r in members(k - LAG_RELAY):
            got(wblk(zi, xl), s_wx.at[r], r_wx.at[r], {"x": xl})
            send(wblk(zi, xl), wblk(zi, xl), s_wx.at[32 + r], r_wx.at[32 + r], {"x": xr})
        for zi, r in members(k - LAG_PAIR):
            got(wblk(zi, xr), s_wx.at[16 + r], r_wx.at[16 + r], {"x": xr})
            got(wblk(zi, x2), s_wx.at[32 + r], r_wx.at[32 + r], {"x": xl})
            send(wg.at[zi, :, c], wg.at[zi, :, c], s_wp.at[r], r_wp.at[r], {"c": other})
        if k == 3:
            got(tg.at[ym, 0], s_t.at[0], r_t.at[0], {"y": ym})
            send(tg.at[ym, 0], tg.at[ym, 0], s_t.at[4], r_t.at[4], {"y": yp})
            got(tg.at[yp, 1], s_t.at[1], r_t.at[1], {"y": yp})
            send(tg.at[yp, 1], tg.at[yp, 1], s_t.at[5], r_t.at[5], {"y": ym})
    for k in range(9):
        for zi, r in members(k):
            got(wg.at[zi, :, other], s_wp.at[r], r_wp.at[r], {"c": other})
    got(tg.at[ym, 1], s_t.at[2], r_t.at[2], {"y": ym})
    got(tg.at[yp, 0], s_t.at[3], r_t.at[3], {"y": yp})
    got(tg.at[y2, 0], s_t.at[4], r_t.at[4], {"y": ym})
    got(tg.at[y2, 1], s_t.at[5], r_t.at[5], {"y": yp})

    rows = 512
    ta = tg[:, 0].reshape(rows, 1024)
    tb = tg[:, 1].reshape(rows, 1024)

    def project(lo, hi):
        wa = wg[0:8, :, :, :, lo:hi].reshape(1024, hi - lo)
        wb = wg[8:16, :, :, :, lo:hi].reshape(1024, hi - lo)
        return jnp.dot(ta, wa, preferred_element_type=F32) + jnp.dot(tb, wb, preferred_element_type=F32)

    glu_s[16 : 16 + rows] = (project(0, 256) * jax.nn.sigmoid(project(256, 512))).astype(BF16)
    kv_s[REACH : REACH + rows] = project(768, 896).astype(BF16)
    send(glu_s.at[16:32], glu_s.at[528:544], s_h.at[0], r_h.at[0], at_sp(prv))
    send(glu_s.at[512:528], glu_s.at[0:16], s_h.at[1], r_h.at[1], at_sp(nxt))
    q_s[...] = (project(512, 768) * 0.125).astype(BF16)
    send(kv_s.at[128:256], kv_s.at[640:768], s_h.at[2], r_h.at[2], at_sp(prv))
    send(kv_s.at[512:640], kv_s.at[0:128], s_h.at[3], r_h.at[3], at_sp(nxt))

    got(glu_s.at[528:544], s_h.at[0], r_h.at[0], at_sp(nxt))
    got(glu_s.at[0:16], s_h.at[1], r_h.at[1], at_sp(prv))
    first = (me > 0).astype(F32)
    last = (me < 127).astype(F32)
    for l in range(2):
        lanes = slice(128 * l, 128 * l + 128)
        padf[l, 0:16] = glu_s[0:16, lanes].astype(F32) * first
        padf[l, 16:528] = glu_s[16:528, lanes].astype(F32)
        padf[l, 528:544] = glu_s[528:544, lanes].astype(F32) * last

    lane64 = lax.broadcasted_iota(jnp.int32, (64, 128), 1)

    def conv_rows(i, carry):
        r0 = i * 64
        accs = []
        for l in range(2):
            lanes = slice(128 * l, 128 * l + 128)
            acc = jnp.broadcast_to(cbias[0:1, lanes], (64, 128))
            for j in range(2 * HALF + 1):
                acc = acc + padf[l, pl.ds(r0 + j + 1, 64), :] * taps[j : j + 1, lanes]
            filt[pl.ds(r0, 64), lanes] = acc
            accs.append(acc)
        s1 = jnp.sum(accs[0] + accs[1], axis=1, keepdims=True)
        s2 = jnp.sum(accs[0] * accs[0] + accs[1] * accs[1], axis=1, keepdims=True)
        stat[pl.ds(r0, 64), :] = jnp.where(lane64 == 0, s1, jnp.where(lane64 == 1, s2, 0.0))
        return carry

    lax.fori_loop(0, 8, conv_rows, 0)
    st_tx[...] = jnp.transpose(stat[...])[0:8, :]

    got(kv_s.at[640:768], s_h.at[2], r_h.at[2], at_sp(nxt))
    got(kv_s.at[0:128], s_h.at[3], r_h.at[3], at_sp(prv))
    kvf = kv_s[...].astype(F32)
    turned = pltpu.roll(kvf, 64, 1)
    low = lax.broadcasted_iota(jnp.int32, (768, 128), 1) < 64
    kvw[0] = jnp.where(low, kvf, 0.0).astype(BF16)
    kvw[1] = jnp.where(low, 0.0, turned).astype(BF16)
    kvw[2] = jnp.where(low, turned, 0.0).astype(BF16)
    kvw[3] = jnp.where(low, 0.0, kvf).astype(BF16)

    for i, dev in enumerate((yp, ym, y2)):
        send(st_tx, st_rx.at[i], s_st.at[i], r_st.at[i], {"y": dev})

    low128 = lax.broadcasted_iota(jnp.int32, (128, 128), 1) < 64
    ends = lax.broadcasted_iota(jnp.int32, (1, 384), 1)

    def attend(i, carry):
        q0 = pl.multiple_of(i * 128, 128)
        pos = me * 512 + i * 128 - REACH + ends
        edge = jnp.where((pos >= 0) & (pos < 65536), 0.0, -1e30).astype(F32)
        bias = mask_s[...] + edge
        for p in range(2):
            qp = q_s[pl.ds(q0, 128), 128 * p : 128 * p + 128]
            probs, inverse = [], []
            for b in range(2):
                h = 2 * p + b
                s = nt_dot(qp, kvw[b, pl.ds(q0, 384), :]) + bias
                top = jnp.maximum(jnp.max(s, axis=1, keepdims=True), sink[h])
                e = jnp.exp(s - top)
                total = jnp.sum(e, axis=1, keepdims=True) + jnp.exp(sink[h] - top)
                log_out[pl.ds(q0, 128), h : h + 1] = top + jnp.log(total)
                probs.append(e.astype(BF16))
                inverse.append(1.0 / total)
            o = jnp.dot(probs[0], kvw[2, pl.ds(q0, 384), :], preferred_element_type=F32)
            o = o + jnp.dot(probs[1], kvw[3, pl.ds(q0, 384), :], preferred_element_type=F32)
            o = o * jnp.where(low128, inverse[0], inverse[1])
            feat[pl.ds(q0, 128), 256 + 128 * p : 384 + 128 * p] = o.astype(BF16)
        return carry

    lax.fori_loop(0, 4, attend, 0)

    for i, dev in enumerate((ym, yp, y2)):
        got(st_rx.at[i], s_st.at[i], r_st.at[i], {"y": dev})
    both = st_tx[...] + st_rx[0] + st_rx[1] + st_rx[2]
    stat[...] = jnp.transpose(jnp.concatenate([both, jnp.zeros((120, 512), F32)], axis=0)) * (1.0 / 1024.0)

    def norm_rows(i, carry):
        r0 = pl.multiple_of(i * 128, 128)
        mean = stat[pl.ds(r0, 128), 0:1]
        var = stat[pl.ds(r0, 128), 1:2] - mean * mean
        v = (filt[pl.ds(r0, 128), :] - mean) * lax.rsqrt(var + 1e-05) * ngain[...] + nbias[...]
        feat[pl.ds(r0, 128), 0:256] = (v * jax.nn.sigmoid(v)).astype(BF16)
        return carry

    lax.fori_loop(0, 4, norm_rows, 0)

    for k in range(9):
        for zi, r in members(k):
            got(og.at[zi, :, other], s_op.at[r], r_op.at[r], {"c": other})

    def out_half(block, half):
        f = feat[pl.ds(pl.multiple_of(block * 128, 128), 128), :]
        return nt_dot(f, og[8 * half : 8 * half + 8].reshape(1024, 512))

    tx2[0] = out_half(y2, 0).astype(BF16)
    tx2[1] = out_half(y2, 1).astype(BF16)
    send(tx2.at[0], rx2.at[0], s_r2.at[0], r_r2.at[0], {"y": yp})
    txp[0, 1] = out_half(yp, 1).astype(BF16)
    send(tx2.at[1], rx2.at[1], s_r2.at[1], r_r2.at[1], {"y": ym})
    txp[1, 0] = out_half(ym, 0).astype(BF16)
    send(txp.at[0, 1], rxp.at[0, 1], s_rp.at[1], r_rp.at[1], {"y": yp})
    part[0] = out_half(yp, 0)
    send(txp.at[1, 0], rxp.at[1, 0], s_rp.at[2], r_rp.at[2], {"y": ym})
    part[1] = out_half(ym, 1)
    part[2] = out_half(y, 0)
    part[3] = out_half(y, 1)
    got(rx2.at[0], s_r2.at[0], r_r2.at[0], {"y": ym})
    txp[0, 0] = (part[0] + rx2[0].astype(F32)).astype(BF16)
    got(rx2.at[1], s_r2.at[1], r_r2.at[1], {"y": yp})
    txp[1, 1] = (part[1] + rx2[1].astype(F32)).astype(BF16)
    send(txp.at[0, 0], rxp.at[0, 0], s_rp.at[0], r_rp.at[0], {"y": yp})
    send(txp.at[1, 1], rxp.at[1, 1], s_rp.at[3], r_rp.at[3], {"y": ym})
    for a, h in ((0, 1), (1, 0), (0, 0), (1, 1)):
        got(rxp.at[a, h], s_rp.at[2 * a + h], r_rp.at[2 * a + h], {"y": ym if a == 0 else yp})
    for h in range(2):
        total = part[2 + h] + rxp[0, h].astype(F32) + rxp[1, h].astype(F32)
        mixed[:, 1024 * h : 1024 * h + 1024] = total.astype(BF16)
    for cp in sent:
        cp.wait_send()


def on_device(
    tokens, in_gain, w_conv_val, w_conv_gate, w_query, w_key, value_weight, conv_taps, conv_bias,
    norm_gain, norm_bias, head_sink_logit, w_out_conv, w_out_attn,
):
    vm = pl.BlockSpec(memory_space=pltpu.VMEM)
    dma = pltpu.SemaphoreType.DMA
    scratch = [
        pltpu.VMEM((16, 4, 2, 16, 896), BF16),
        pltpu.VMEM((16, 4, 2, 16, 512), BF16),
        pltpu.VMEM((4, 2, 128, 1024), BF16),
        pltpu.VMEM((544, 256), BF16),
        pltpu.VMEM((512, 256), BF16),
        pltpu.VMEM((768, 128), BF16),
        pltpu.VMEM((4, 768, 128), BF16),
        pltpu.VMEM((2, 544, 128), F32),
        pltpu.VMEM((512, 256), F32),
        pltpu.VMEM((512, 128), F32),
        pltpu.VMEM((8, 512), F32),
        pltpu.VMEM((3, 8, 512), F32),
        pltpu.VMEM((512, 512), BF16),
        pltpu.VMEM((128, 384), F32),
        pltpu.VMEM((4, 128, 1024), F32),
        pltpu.VMEM((2, 128, 1024), BF16),
        pltpu.VMEM((2, 128, 1024), BF16),
        pltpu.VMEM((2, 2, 128, 1024), BF16),
        pltpu.VMEM((2, 2, 128, 1024), BF16),
    ]
    for n in (16, 48, 16, 3, 32, 16, 6, 4, 3, 2, 4):
        scratch += [dma((n,)), dma((n,))]
    return pl.pallas_call(
        layer,
        name="layer",
        out_shape=(
            jax.ShapeDtypeStruct((128, 2048), BF16),
            jax.ShapeDtypeStruct((512, 4), F32),
        ),
        in_specs=[vm] * 13 + [pl.BlockSpec(memory_space=pltpu.SMEM)],
        out_specs=(vm, vm),
        scratch_shapes=scratch,
        compiler_params=pltpu.CompilerParams(
            collective_id=0, has_side_effects=True, vmem_limit_bytes=56 * 1024 * 1024
        ),
    )(
        tokens, in_gain[None], w_conv_val, w_conv_gate, w_query, w_key, value_weight,
        w_out_conv, w_out_attn, conv_taps, conv_bias[None], norm_gain[None], norm_bias[None],
        head_sink_logit,
    )


def solution(mesh):
    finer = Mesh(mesh.devices.reshape(16, 4, 2, mesh.shape["tp"]), ("z", "x", "c", "y"))
    in_specs = (
        P(SP_TP, None), P(),
        P(SP, "y"), P(SP, "y"), P(SP, "y"), P(SP, "y"), P(SP, "y"),
        P(None, "y"), P("y"), P("y"), P("y"), P("y"),
        P("y", SP), P("y", SP),
    )
    return jax.shard_map(
        on_device, mesh=finer, in_specs=in_specs, out_specs=(P(SP_TP, None), P(SP, "y")), check_vma=False
    )
```

time: 240 us -> 93.2 us (0.39)
  waiting for transfers between devices: 143 us -> 0 us
  Pallas kernels: 0 us -> 85.6 us
  starting transfers between devices: 40.8 us -> 0 us
  between operations: 14.3 us -> 0.65 us
  matrix products: 11 us -> 0 us
  other arithmetic: 10.9 us -> 0 us
  blocking collectives: 9.68 us -> 0 us
    all_to_all x4 -> x0, waiting for transfers between devices: 99.1 us -> none  [the longest x3 74.8 us: from_everyone(): return lax.all_to_all(copies, axis, split_axis=0, concat_axis=0, tiled=True)]
    pallas_call x0 -> x1, Pallas kernels: none -> 85.6 us  [on_device(): pl.pallas_call(layer, name='layer', out_shape=(jax.ShapeDtypeStruct((128,...]
    all_gather x1 -> x0, waiting for transfers between devices: 38.2 us -> none  [sent_together(): filled = lax.all_gather(both, axis, axis=dim, tiled=True)]
    all_to_all x4 -> x0, starting transfers between devices: 31.9 us -> none  [the longest x3 27.4 us: from_everyone(): return lax.all_to_all(copies, axis, split_axis=0, concat_axis=0, tiled=True)]
    dot_general x4 -> x0, matrix products: 11 us -> none  [the longest x1 5.01 us: on_device(): jnp.dot(gather_directly(normed, 'tp', 0), joined, preferred_element_type=...]
    all_to_all x1 -> x0, blocking collectives: 9.68 us -> none  [from_everyone(): return lax.all_to_all(copies, axis, split_axis=0, concat_axis=0, tiled=True)]
    ppermute x4 -> x0, starting transfers between devices: 8.83 us -> none  [the longest x2 4.63 us: with_halo(): lax.ppermute(head, axis, [((i + 1) % count, i) for i in range(ends)])]
    reduce_sum x5 -> x0, other arithmetic: 6.8 us -> none  [the longest x1 2.68 us: on_device(): jnp.sum(filtered, axis=-1)]
  transfers between devices with their start and end apart: 9 -> 0, of which waited for: 6 -> 0; matrix products, arithmetic and copies ran while one was open for 5% -> 0% of each run, Pallas kernels for 0% -> 0%
where the time goes in v1:
time: 93.2 us; the launch traced here: 92 us
  Pallas kernels  85.6 us (92%)
  local copies, waits for them, and re-layouts  5.7 us (6%)
    pallas_call x1, Pallas kernels, on_device(): pl.pallas_call(layer, name='layer', out_shape=(jax.ShapeDtypeStruct((128,...  85.6 us
    unnamed x5, local copies, waits for them, and re-layouts  4.04 us

profile of v1, /device:TPU:1, one launch (start us, length us, event | category | flops | bytes accessed | tf_op | source)
XLA Modules:
  0.0 92.0 jit_solution(1880651889333737535)
XLA Ops:
  0.6 0.0 copy-start
  0.6 1.4 %copy.16.w_oc = bf16[256,16]{1,0:T(8,128)(2,1)} copy(bf16[256,16]{0,1:T(8,128)(2,1)} %param.26) | data formatting | bytes 16384 | tf_op args[12]
  2.1 0.0 copy-done
  2.1 0.7 copy.17.w_oa
  2.8 85.6 %layer.1 = (bf16[128,2048]{1,0:T(8,128)(2,1)}, f32[512,4]{1,0:T(8,128)}) custom-call(bf16[128,2048]{1,0:T(8,128)(2,1)} %tok.1, f32[1,2048]{1,0:T(1,128)} %bitcast.4, bf16[16,256]{1,0:T(8,128)(2,1)} %w_val.1, bf16[16,256]{1,0:T(8,128)(2,1)} %w_gate.1, bf16[16,256]{1,0:T(8,128)(2,1)} %w_q.1, bf16[16,64]{1,0:T(8,128)(2,1)} %w_k.1, bf16[16,64]{1,0:T(8,128)(2,1)} %w_v.1, ...), custom_call_target="tpu_custom_call" | custom-call | tf_op jit(solution)/shard_map/layer/pallas_call | solution.py:348
  88.4 1.7 %copy.18 = f32[512,4]{0,1:T(4,128)} copy(f32[512,4]{1,0:T(8,128)} %get-tuple-element.3) | data formatting | bytes 16384 | tf_op jit(solution)/shard_map/layer/pallas_call | solution.py:348
  90.1 1.9 %copy.20 = bf16[128,2048]{1,0:T(8,128)(2,1)} copy(bf16[128,2048]{1,0:T(8,128)(2,1)} %get-tuple-element.6) | data formatting | bytes 1048576
Async XLA Ops:
  0.6 1.4 %copy-start = (bf16[256,16]{0,1:T(8,128)(2,1)S(1)}, bf16[256,16]{0,1:T(8,128)(2,1)}, u32[]{:S(2)}) copy-start(bf16[256,16]{0,1:T(8,128)(2,1)} %param.27) | copy-start | bytes 24580

commit v2 on v1

v2 whole, which is shorter than its diff:
```python
import jax
import jax.numpy as jnp
from jax import lax
from jax.experimental import pallas as pl
from jax.experimental.pallas import tpu as pltpu
from jax.sharding import Mesh
from jax.sharding import PartitionSpec as P

MESH = pl.DeviceIdType.MESH
REACH = 128
HEADS = 4
HALF = 15
F32 = jnp.float32
BF16 = jnp.bfloat16
SP = ("z", "x", "c")
SP_TP = ("z", "x", "c", "y")


def nt_dot(a, b):
    return lax.dot_general(a, b, (((1,), (1,)), ((), ())), preferred_element_type=F32)


def layer(
    tok_h, gain_h, val_h, gate_h, wq_h, wk_h, wv_h, oc_h, oa_h, taps_h, cbias_h, ngain_h, nbias_h, sink,
    mixed, log_out,
    tok, gain, wk, wv, taps, cbias, ngain, nbias,
    wg, og, tg, glu_s, q_s, kv_s, kvw, padf, filt, stat, lstat, st_tx, st_rx, feat, mask_s,
    part, tx2, rx2, txp, rxp, s_in,
    r_wz, r_wx, r_wg, r_wp, r_ox, r_oz, r_on, r_op, r_t, r_h, r_st, r_r2, r_rp, out_sem,
):
    z, x, c, y = (lax.axis_index(n) for n in ("z", "x", "c", "y"))
    d = 1 - 2 * c

    def along(e):
        return lax.rem(z + 16 + e, 16)

    xr, xl = lax.rem(x + 4 + d, 4), lax.rem(x + 4 - d, 4)
    x2 = lax.rem(x + 2, 4)
    yp, ym, y2 = lax.rem(y + 1, 4), lax.rem(y + 3, 4), lax.rem(y + 2, 4)
    other = 1 - c
    me = z * 8 + x * 2 + c
    nxt, prv = lax.rem(me + 1, 128), lax.rem(me + 127, 128)

    def at_sp(s):
        return {"z": s // 8, "x": lax.rem(s // 2, 4), "c": lax.rem(s, 2)}

    def copy(src, dst, ssem, rsem, dev):
        return pltpu.make_async_remote_copy(
            src_ref=src, dst_ref=dst, send_sem=ssem, recv_sem=rsem,
            device_id=dev, device_id_type=MESH,
        )

    open_scope = []

    def phase(name):
        if open_scope:
            open_scope.pop().__exit__(None, None, None)
        if name:
            scope = jax.named_scope(name)
            scope.__enter__()
            open_scope.append(scope)

    def send(src, dst, ssem, rsem, dev):
        copy(src, dst, ssem, rsem, dev).start()

    def got(dst, ssem, rsem, dev):
        copy(dst, dst, ssem, rsem, dev).wait_recv()

    phase("greet")
    barrier = pltpu.get_barrier_semaphore()
    greet = [{"z": along(e)} for e in (1, -1, 2, -2, 4, -4, 8)]
    greet += [{"x": xr}, {"x": xl}, {"c": other}, {"y": yp}, {"y": ym}, {"y": y2}, at_sp(nxt), at_sp(prv)]
    for dev in greet:
        pl.semaphore_signal(barrier, inc=1, device_id=dev, device_id_type=MESH)

    wown, oown = wg.at[z, x, c], og.at[z, x, c]
    loads = [
        pltpu.make_async_copy(src, dst, s_in.at[i])
        for i, (src, dst) in enumerate((
            (tok_h, tok), (gain_h, gain), (wk_h, wk), (wv_h, wv),
            (val_h, wown.at[:, 0:256]), (gate_h, wown.at[:, 256:512]), (wq_h, wown.at[:, 512:768]),
            (oc_h, oown.at[:, 0:256]), (oa_h, oown.at[:, 256:512]),
            (taps_h, taps), (cbias_h, cbias), (ngain_h, ngain), (nbias_h, nbias),
        ))
    ]
    for cp in loads:
        cp.start()
    row = lax.broadcasted_iota(jnp.int32, (128, 384), 0)
    col = lax.broadcasted_iota(jnp.int32, (128, 384), 1)
    mask_s[...] = jnp.where((col >= row) & (col <= row + 2 * REACH), 0.0, -1e30).astype(F32)
    for cp in loads[2:4]:
        cp.wait()
    wg[z, x, c, :, 768:896] = jnp.concatenate([wk[...], wv[...]], axis=1)
    for cp in loads[0:2]:
        cp.wait()
    t = tok[...].astype(F32)
    inv = lax.rsqrt(jnp.mean(t * t, axis=-1, keepdims=True) + 1e-06)
    normed = (t * inv * gain[...]).astype(BF16)
    tg[y, 0] = normed[:, :1024]
    tg[y, 1] = normed[:, 1024:]
    for cp in loads[4:]:
        cp.wait()

    phase("barrier")
    pl.semaphore_wait(barrier, len(greet))
    phase("start")

    def source(r, way):
        return lax.rem(z + 16 + 4 * (r // 4) + (0, -1, 1, -2 * way)[r % 4], 16)

    def sender(j):
        return {"z": along((0, -1, 1, -2 * d)[j])}

    def wblk(r, xi):
        return wg.at[source(r, d), xi, c]

    def w_far():
        for i, e in ((1, -4), (3, 4), (2, 8)):
            send(wown, wown, out_sem.at[0], r_wz.at[4 * i], {"z": along(e)})

    def w_near(i):
        blk = wblk(4 * i, x)
        for j, e in ((1, 1), (2, -1), (3, 2 * d)):
            send(blk, blk, out_sem.at[0], r_wz.at[4 * i + j], {"z": along(e)})

    def w_arrive(r):
        dev = sender(r % 4) if r % 4 else {"z": along(4 * (r // 4))}
        got(wblk(r, x), out_sem.at[0], r_wz.at[r], dev)

    groups = ((0,), (1, 2, 3), (4, 12, 8), (5, 6, 7), (13, 14, 15), (9, 10, 11))

    def group_of(r):
        return [r in g for g in groups].index(True)

    def w_side(r):
        send(wblk(r, x), wblk(r, x), out_sem.at[1], r_wx.at[r], {"x": xr})
        send(wblk(r, x), wblk(r, x), out_sem.at[1], r_wg.at[group_of(r)], {"x": xl})

    def w_relay(r):
        got(wblk(r, xl), out_sem.at[1], r_wx.at[r], {"x": xl})
        send(wblk(r, xl), wblk(r, xl), out_sem.at[1], r_wg.at[6 + group_of(r)], {"x": xr})

    def w_pairs(*gs):
        for g in gs:
            some = wg.at[0, 0 : len(groups[g]), 0]
            got(some, out_sem.at[1], r_wg.at[g], {"x": xr})
            got(some, out_sem.at[1], r_wg.at[6 + g], {"x": xl})
            for r in groups[g]:
                both = wg.at[source(r, d), :, c]
                send(both, both, out_sem.at[2], r_wp.at[0], {"c": other})

    def oblk(i, xi):
        return og.at[source(4 * i, d), xi, c]

    def o_far():
        for i, e in ((1, -4), (3, 4), (2, 8)):
            send(oown, oown, out_sem.at[12], r_oz.at[i], {"z": along(e)})

    def o_side(i):
        if i:
            got(oblk(i, x), out_sem.at[12], r_oz.at[i], {"z": along(4 * i)})
        send(oblk(i, x), oblk(i, x), out_sem.at[3], r_ox.at[i], {"x": xr})
        send(oblk(i, x), oblk(i, x), out_sem.at[3], r_ox.at[4 + i], {"x": xl})

    def o_relay(i):
        got(oblk(i, xl), out_sem.at[3], r_ox.at[i], {"x": xl})
        send(oblk(i, xl), oblk(i, xl), out_sem.at[3], r_ox.at[8 + i], {"x": xr})

    def o_pair(r):
        four = og.at[source(r, d), :, c]
        send(four, four, out_sem.at[5], r_op.at[0], {"c": other})

    def o_near(i):
        got(oblk(i, xr), out_sem.at[3], r_ox.at[4 + i], {"x": xr})
        got(oblk(i, x2), out_sem.at[3], r_ox.at[8 + i], {"x": xl})
        four = og.at[source(4 * i, d), :, c]
        for j, e in ((1, 1), (2, -1), (3, 2 * d)):
            send(four, four, out_sem.at[4], r_on.at[i], {"z": along(e)})
        o_pair(4 * i)

    def o_last(i):
        got(og.at[0:3, :, 0], out_sem.at[4], r_on.at[i], sender(1))
        for j in (1, 2, 3):
            o_pair(4 * i + j)

    o_plan = (
        (o_far, lambda: o_side(0)),
        (lambda: o_side(1), lambda: o_side(3)),
        (lambda: o_side(2), lambda: o_near(0)),
        (lambda: o_relay(1), lambda: o_relay(3), lambda: o_relay(2)),
        (lambda: o_near(1), lambda: o_near(3)),
        (lambda: o_near(2),),
        (lambda: o_last(0),),
        (lambda: o_last(1), lambda: o_last(3)),
        (lambda: o_last(2),),
    )

    def o_step(n):
        for act in o_plan[n]:
            act()

    def w_arrivals(*rs):
        for r in rs:
            w_arrive(r)
            if r % 4 == 0:
                w_near(r // 4)
            w_side(r)

    def w_relays(*rs):
        for r in rs:
            w_relay(r)

    w_near(0)
    w_side(0)
    w_far()
    send(tg.at[y, 0], tg.at[y, 0], out_sem.at[6], r_t.at[0], {"y": yp})
    send(tg.at[y, 1], tg.at[y, 1], out_sem.at[6], r_t.at[1], {"y": ym})
    send(tg.at[y, 1], tg.at[y, 1], out_sem.at[6], r_t.at[2], {"y": yp})
    send(tg.at[y, 0], tg.at[y, 0], out_sem.at[6], r_t.at[3], {"y": ym})
    phase("arrA")
    w_arrivals(1, 2, 3)
    phase("relB")
    w_relays(0)
    phase("arrC")
    w_arrivals(4, 12)
    o_step(0)
    phase("arrE")
    w_arrivals(8)
    phase("relF")
    w_relays(1, 2, 3)
    o_relay(0)
    phase("arrH")
    w_arrivals(5, 6, 7, 13, 14, 15)
    phase("tok")
    got(tg.at[ym, 0], out_sem.at[6], r_t.at[0], {"y": ym})
    send(tg.at[ym, 0], tg.at[ym, 0], out_sem.at[6], r_t.at[4], {"y": yp})
    got(tg.at[yp, 1], out_sem.at[6], r_t.at[1], {"y": yp})
    send(tg.at[yp, 1], tg.at[yp, 1], out_sem.at[6], r_t.at[5], {"y": ym})
    phase("relI")
    w_relays(4, 12, 8)
    phase("arrK")
    w_arrivals(9, 10, 11)
    phase("o1")
    o_step(1)
    phase("pairL")
    w_pairs(0, 1)
    phase("relL")
    w_relays(5, 6, 7, 13, 14, 15)
    phase("o2")
    o_step(2)
    phase("pairM")
    w_pairs(2)
    phase("relM")
    w_relays(9, 10, 11)
    phase("pairN")
    w_pairs(3, 4)
    phase("o3")
    o_step(3)
    phase("pairO")
    w_pairs(5)
    phase("o4")
    o_step(4)
    phase("waitpair")
    got(wg.at[0:8], out_sem.at[2], r_wp.at[0], {"c": other})
    phase("waittok")
    got(tg.at[ym, 1], out_sem.at[6], r_t.at[2], {"y": ym})
    got(tg.at[yp, 0], out_sem.at[6], r_t.at[3], {"y": yp})
    got(tg.at[y2, 0], out_sem.at[6], r_t.at[4], {"y": ym})
    got(tg.at[y2, 1], out_sem.at[6], r_t.at[5], {"y": yp})
    o_left = list(range(5, len(o_plan)))

    def o_service(count=1):
        for _ in range(count):
            if o_left:
                o_step(o_left.pop(0))

    phase("proj")
    rows = 512
    ta = tg[:, 0].reshape(rows, 1024)
    tb = tg[:, 1].reshape(rows, 1024)

    def project(lo, hi):
        wa = wg[0:8, :, :, :, lo:hi].reshape(1024, hi - lo)
        wb = wg[8:16, :, :, :, lo:hi].reshape(1024, hi - lo)
        return jnp.dot(ta, wa, preferred_element_type=F32) + jnp.dot(tb, wb, preferred_element_type=F32)

    qkv = project(512, 896)
    kv_s[REACH : REACH + rows] = qkv[:, 256:].astype(BF16)
    q_s[...] = (qkv[:, :256] * 0.125).astype(BF16)
    phase("service1")
    o_service()
    phase("projglu")
    send(kv_s.at[128:256], kv_s.at[640:768], out_sem.at[11], r_h.at[2], at_sp(prv))
    send(kv_s.at[512:640], kv_s.at[0:128], out_sem.at[11], r_h.at[3], at_sp(nxt))
    glu = (project(0, 256) * jax.nn.sigmoid(project(256, 512))).astype(BF16)
    glu_s[16 : 16 + rows] = glu
    for l in range(2):
        padf[l, 16:528] = glu[:, 128 * l : 128 * l + 128].astype(F32)
    phase("service2")
    o_service()
    send(glu_s.at[16:32], glu_s.at[528:544], out_sem.at[7], r_h.at[0], at_sp(prv))
    send(glu_s.at[512:528], glu_s.at[0:16], out_sem.at[7], r_h.at[1], at_sp(nxt))

    lane64 = lax.broadcasted_iota(jnp.int32, (64, 128), 1)

    def conv_rows(i, carry):
        r0 = i * 64
        accs = []
        for l in range(2):
            lanes = slice(128 * l, 128 * l + 128)
            acc = jnp.broadcast_to(cbias[0:1, lanes], (64, 128))
            for j in range(2 * HALF + 1):
                acc = acc + padf[l, pl.ds(r0 + j + 1, 64), :] * taps[j : j + 1, lanes]
            filt[pl.ds(r0, 64), lanes] = acc
            accs.append(acc)
        s1 = jnp.sum(accs[0] + accs[1], axis=1, keepdims=True)
        s2 = jnp.sum(accs[0] * accs[0] + accs[1] * accs[1], axis=1, keepdims=True)
        stat[pl.ds(r0, 64), :] = jnp.where(lane64 == 0, s1, jnp.where(lane64 == 1, s2, 0.0))
        return carry

    phase("conv")
    lax.fori_loop(1, 7, conv_rows, 0)
    phase("service3")
    o_service()
    phase("waithalo")
    got(glu_s.at[528:544], out_sem.at[7], r_h.at[0], at_sp(nxt))
    got(glu_s.at[0:16], out_sem.at[7], r_h.at[1], at_sp(prv))
    phase("conv2")
    first = (me > 0).astype(F32)
    last = (me < 127).astype(F32)
    for l in range(2):
        lanes = slice(128 * l, 128 * l + 128)
        padf[l, 0:16] = glu_s[0:16, lanes].astype(F32) * first
        padf[l, 528:544] = glu_s[528:544, lanes].astype(F32) * last
    conv_rows(0, 0)
    conv_rows(7, 0)
    st_tx[...] = jnp.transpose(stat[...])[0:8, :]

    phase("waitkv")
    got(kv_s.at[640:768], out_sem.at[11], r_h.at[2], at_sp(nxt))
    got(kv_s.at[0:128], out_sem.at[11], r_h.at[3], at_sp(prv))
    for i, dev in enumerate((yp, ym, y2)):
        send(st_tx, st_rx.at[i], out_sem.at[8], r_st.at[0], {"y": dev})
    phase("kvprep")
    kvf = kv_s[...].astype(F32)
    turned = pltpu.roll(kvf, 64, 1)
    low = lax.broadcasted_iota(jnp.int32, (768, 128), 1) < 64
    kvw[0] = jnp.where(low, kvf, 0.0).astype(BF16)
    kvw[1] = jnp.where(low, 0.0, turned).astype(BF16)
    kvw[2] = jnp.where(low, turned, 0.0).astype(BF16)
    kvw[3] = jnp.where(low, 0.0, kvf).astype(BF16)

    phase("attend")
    low128 = lax.broadcasted_iota(jnp.int32, (128, 128), 1) < 64
    ends = lax.broadcasted_iota(jnp.int32, (1, 384), 1)

    def attend(i):
        q0 = pl.multiple_of(i * 128, 128)
        pos = me * 512 + i * 128 - REACH + ends
        edge = jnp.where((pos >= 0) & (pos < 65536), 0.0, -1e30).astype(F32)
        bias = mask_s[...] + edge
        for p in range(2):
            qp = q_s[pl.ds(q0, 128), 128 * p : 128 * p + 128]
            probs, inverse = [], []
            for b in range(2):
                h = 2 * p + b
                s = nt_dot(qp, kvw[b, pl.ds(q0, 384), :]) + bias
                top = jnp.maximum(jnp.max(s, axis=1, keepdims=True), sink[h])
                e = jnp.exp(s - top)
                total = jnp.sum(e, axis=1, keepdims=True) + jnp.exp(sink[h] - top)
                lstat[pl.ds(q0, 128), h : h + 1] = top + jnp.log(total)
                probs.append(e.astype(BF16))
                inverse.append(1.0 / total)
            o = jnp.dot(probs[0], kvw[2, pl.ds(q0, 384), :], preferred_element_type=F32)
            o = o + jnp.dot(probs[1], kvw[3, pl.ds(q0, 384), :], preferred_element_type=F32)
            o = o * jnp.where(low128, inverse[0], inverse[1])
            feat[pl.ds(q0, 128), 256 + 128 * p : 384 + 128 * p] = o.astype(BF16)

    order = (y2, yp, ym, y)
    for n in range(3):
        phase(f"attend{n}")
        attend(order[n])
        phase(f"service{n + 4}")
        o_service()
    o_service(len(o_left))
    phase("waitstat")
    got(st_rx, out_sem.at[8], r_st.at[0], {"y": ym})
    phase("norm")
    both = st_tx[...] + st_rx[0] + st_rx[1] + st_rx[2]
    stat[...] = jnp.transpose(jnp.concatenate([both, jnp.zeros((120, 512), F32)], axis=0)) * (1.0 / 1024.0)

    def norm_rows(i):
        r0 = pl.multiple_of(i * 128, 128)
        mean = stat[pl.ds(r0, 128), 0:1]
        var = stat[pl.ds(r0, 128), 1:2] - mean * mean
        v = (filt[pl.ds(r0, 128), :] - mean) * lax.rsqrt(var + 1e-05) * ngain[...] + nbias[...]
        feat[pl.ds(r0, 128), 0:256] = (v * jax.nn.sigmoid(v)).astype(BF16)

    norm_rows(y2)

    phase("waitout")
    got(og.at[0:8], out_sem.at[5], r_op.at[0], {"c": other})

    def out_half(block, half):
        f = feat[pl.ds(pl.multiple_of(block * 128, 128), 128), :]
        return nt_dot(f, og[8 * half : 8 * half + 8].reshape(1024, 512))

    phase("outmm")
    tx2[0] = out_half(y2, 0).astype(BF16)
    tx2[1] = out_half(y2, 1).astype(BF16)
    send(tx2.at[0], rx2.at[0], out_sem.at[9], r_r2.at[0], {"y": yp})
    norm_rows(yp)
    send(tx2.at[1], rx2.at[1], out_sem.at[9], r_r2.at[1], {"y": ym})
    norm_rows(ym)
    txp[0, 1] = out_half(yp, 1).astype(BF16)
    txp[1, 0] = out_half(ym, 0).astype(BF16)
    send(txp.at[0, 1], rxp.at[0, 1], out_sem.at[10], r_rp.at[1], {"y": yp})
    part[0] = out_half(yp, 0)
    send(txp.at[1, 0], rxp.at[1, 0], out_sem.at[10], r_rp.at[2], {"y": ym})
    part[1] = out_half(ym, 1)
    phase("attendown")
    attend(y)
    norm_rows(y)
    part[2] = out_half(y, 0)
    part[3] = out_half(y, 1)
    phase("wait2")
    got(rx2.at[0], out_sem.at[9], r_r2.at[0], {"y": ym})
    txp[0, 0] = (part[0] + rx2[0].astype(F32)).astype(BF16)
    got(rx2.at[1], out_sem.at[9], r_r2.at[1], {"y": yp})
    txp[1, 1] = (part[1] + rx2[1].astype(F32)).astype(BF16)
    send(txp.at[0, 0], rxp.at[0, 0], out_sem.at[10], r_rp.at[0], {"y": yp})
    send(txp.at[1, 1], rxp.at[1, 1], out_sem.at[10], r_rp.at[3], {"y": ym})
    phase("waitfin")
    log_out[...] = jnp.transpose(lstat[...])[0:4, :]
    for a, h in ((0, 1), (1, 0), (0, 0), (1, 1)):
        got(rxp.at[a, h], out_sem.at[10], r_rp.at[2 * a + h], {"y": ym if a == 0 else yp})
    phase("final")
    for h in range(2):
        total = part[2 + h] + rxp[0, h].astype(F32) + rxp[1, h].astype(F32)
        mixed[:, 1024 * h : 1024 * h + 1024] = total.astype(BF16)
    phase("drain")
    for i, ref in enumerate((
        wg.at[0:5, 0:3, 0], wg.at[0:6], wg.at[0:8], og.at[0:3, :, 0], og.at[0:6], og.at[0:8], tg.at[0:3],
        glu_s.at[0:32], st_rx, tx2, txp, kv_s.at[0:256], og.at[0:3, 0, 0],
    )):
        copy(ref, ref, out_sem.at[i], r_wp.at[0], {"c": other}).wait_send()
    phase(None)


def on_device(
    tokens, in_gain, w_conv_val, w_conv_gate, w_query, w_key, value_weight, conv_taps, conv_bias,
    norm_gain, norm_bias, head_sink_logit, w_out_conv, w_out_attn,
):
    vm = pl.BlockSpec(memory_space=pltpu.VMEM)
    dma = pltpu.SemaphoreType.DMA
    scratch = [
        pltpu.VMEM((128, 2048), BF16),
        pltpu.VMEM((1, 2048), F32),
        pltpu.VMEM((16, 64), BF16),
        pltpu.VMEM((16, 64), BF16),
        pltpu.VMEM((31, 256), F32),
        pltpu.VMEM((1, 256), F32),
        pltpu.VMEM((1, 256), F32),
        pltpu.VMEM((1, 256), F32),
        pltpu.VMEM((16, 4, 2, 16, 896), BF16),
        pltpu.VMEM((16, 4, 2, 16, 512), BF16),
        pltpu.VMEM((4, 2, 128, 1024), BF16),
        pltpu.VMEM((544, 256), BF16),
        pltpu.VMEM((512, 256), BF16),
        pltpu.VMEM((768, 128), BF16),
        pltpu.VMEM((4, 768, 128), BF16),
        pltpu.VMEM((2, 544, 128), F32),
        pltpu.VMEM((512, 256), F32),
        pltpu.VMEM((512, 128), F32),
        pltpu.VMEM((512, 128), F32),
        pltpu.VMEM((8, 512), F32),
        pltpu.VMEM((3, 8, 512), F32),
        pltpu.VMEM((512, 512), BF16),
        pltpu.VMEM((128, 384), F32),
        pltpu.VMEM((4, 128, 1024), F32),
        pltpu.VMEM((2, 128, 1024), BF16),
        pltpu.VMEM((2, 128, 1024), BF16),
        pltpu.VMEM((2, 2, 128, 1024), BF16),
        pltpu.VMEM((2, 2, 128, 1024), BF16),
        dma((13,)),
    ]
    for n in (16, 16, 12, 1, 12, 4, 4, 1, 6, 4, 1, 2, 4, 13):
        scratch += [dma((n,))]
    mixed, log_total = pl.pallas_call(
        layer,
        name="layer",
        out_shape=(
            pltpu.VMEM((128, 2048), BF16),
            pltpu.VMEM((4, 512), F32),
        ),
        in_specs=[pl.BlockSpec(memory_space=pl.ANY)] * 13 + [pl.BlockSpec(memory_space=pltpu.SMEM)],
        out_specs=(vm, vm),
        scratch_shapes=scratch,
        compiler_params=pltpu.CompilerParams(
            collective_id=0, has_side_effects=True, vmem_limit_bytes=56 * 1024 * 1024
        ),
    )(
        tokens, in_gain[None], w_conv_val, w_conv_gate, w_query, w_key, value_weight,
        w_out_conv.T, w_out_attn.T, conv_taps, conv_bias[None], norm_gain[None], norm_bias[None],
        head_sink_logit,
    )
    return mixed, log_total.T


def solution(mesh):
    finer = Mesh(mesh.devices.reshape(16, 4, 2, mesh.shape["tp"]), ("z", "x", "c", "y"))
    in_specs = (
        P(SP_TP, None), P(),
        P(SP, "y"), P(SP, "y"), P(SP, "y"), P(SP, "y"), P(SP, "y"),
        P(None, "y"), P("y"), P("y"), P("y"), P("y"),
        P("y", SP), P("y", SP),
    )
    return jax.shard_map(
        on_device, mesh=finer, in_specs=in_specs, out_specs=(P(SP_TP, None), P(SP, "y")), check_vma=False
    )
```

time: 93.2 us -> 78.6 us (0.84)
  Pallas kernels: 85.6 us -> 75.6 us
  local copies, waits for them, and re-layouts: 5.7 us -> 1.39 us
    pallas_call x1, Pallas kernels: 85.6 us -> 75.6 us  [on_device(): pl.pallas_call(layer, name='layer', out_shape=(pltpu.VMEM((128, 2048), BF...]
    unnamed x5 -> x2, local copies, waits for them, and re-layouts: 4.04 us -> 1.39 us
    pallas_call x1 -> x0, local copies, waits for them, and re-layouts: 1.66 us -> none  [on_device(): pl.pallas_call(layer, name='layer', out_shape=(jax.ShapeDtypeStruct((128,...]
where the time goes in v2:
time: 78.6 us; the launch traced here: 77.6 us
  Pallas kernels  75.6 us (96%)
  local copies, waits for them, and re-layouts  1.39 us (2%)
    pallas_call x1, Pallas kernels, on_device(): pl.pallas_call(layer, name='layer', out_shape=(pltpu.VMEM((128, 2048), BF...  75.6 us

profile of v2, /device:TPU:1, one launch (start us, length us, event | category | flops | bytes accessed | tf_op | source)
XLA Modules:
  0.0 77.6 jit_solution(4201104515933936473)
XLA Ops:
  0.6 75.6 %layer.1 = (bf16[128,2048]{1,0:T(8,128)(2,1)S(1)}, f32[4,512]{1,0:T(4,128)S(1)}) custom-call(bf16[128,2048]{1,0:T(8,128)(2,1)} %tok_h.1, f32[1,2048]{1,0:T(1,128)} %bitcast.8, bf16[16,256]{1,0:T(8,128)(2,1)} %val_h.1, bf16[16,256]{1,0:T(8,128)(2,1)} %gate_h.1, bf16[16,256]{1,0:T(8,128)(2,1)} %wq_h.1, bf16[16,64]{1,0:T(8,128)(2,1)} %wk_h.1, ...), custom_call_target="tpu_custom_call" | custom-call | tf_op jit(solution)/shard_map/layer/pallas_call | solution.py:489
  76.2 0.8 %copy.18 = bf16[128,2048]{1,0:T(8,128)(2,1)} copy(bf16[128,2048]{1,0:T(8,128)(2,1)S(1)} %get-tuple-element.6) | data formatting | bytes 1048576
  77.0 0.6 copy.19

commit v3 on v2

--- a/solution.py
+++ b/solution.py
@@ -21,11 +21,11 @@
 
 
 def layer(
-    tok_h, gain_h, val_h, gate_h, wq_h, wk_h, wv_h, oc_h, oa_h, taps_h, cbias_h, ngain_h, nbias_h, sink,
+    tok_h, gain_h, val_h, gate_h, wq_h, wk_h, wv_h, oc_h, oa_h, taps_h, cbias_h, ngain_h, nbias_h, sink_h,
     mixed, log_out,
-    tok, gain, wk, wv, taps, cbias, ngain, nbias,
+    tok, gain, wk, wv, taps, cbias, ngain, nbias, sink,
     wg, og, tg, glu_s, q_s, kv_s, kvw, padf, filt, stat, lstat, st_tx, st_rx, feat, mask_s,
-    part, tx2, rx2, txp, rxp, s_in,
+    part, tx2, rx2, tx4, rx4, s_in,
     r_wz, r_wx, r_wg, r_wp, r_ox, r_oz, r_on, r_op, r_t, r_h, r_st, r_r2, r_rp, out_sem,
 ):
     z, x, c, y = (lax.axis_index(n) for n in ("z", "x", "c", "y"))
@@ -68,7 +68,7 @@
 
     phase("greet")
     barrier = pltpu.get_barrier_semaphore()
-    greet = [{"z": along(e)} for e in (1, -1, 2, -2, 4, -4, 8)]
+    greet = [{"z": along(e)} for e in (1, -1, 2, -2, 4, -4)]
     greet += [{"x": xr}, {"x": xl}, {"c": other}, {"y": yp}, {"y": ym}, {"y": y2}, at_sp(nxt), at_sp(prv)]
     for dev in greet:
         pl.semaphore_signal(barrier, inc=1, device_id=dev, device_id_type=MESH)
@@ -80,7 +80,7 @@
             (tok_h, tok), (gain_h, gain), (wk_h, wk), (wv_h, wv),
             (val_h, wown.at[:, 0:256]), (gate_h, wown.at[:, 256:512]), (wq_h, wown.at[:, 512:768]),
             (oc_h, oown.at[:, 0:256]), (oa_h, oown.at[:, 256:512]),
-            (taps_h, taps), (cbias_h, cbias), (ngain_h, ngain), (nbias_h, nbias),
+            (taps_h, taps), (cbias_h, cbias), (ngain_h, ngain), (nbias_h, nbias), (sink_h, sink),
         ))
     ]
     for cp in loads:
@@ -115,8 +115,12 @@
         return wg.at[source(r, d), xi, c]
 
     def w_far():
-        for i, e in ((1, -4), (3, 4), (2, 8)):
+        for i, e in ((1, -4), (3, 4)):
             send(wown, wown, out_sem.at[0], r_wz.at[4 * i], {"z": along(e)})
+
+    def w_farther():
+        blk = wg.at[along(-4 * d), x, c]
+        send(blk, blk, out_sem.at[0], r_wz.at[8], {"z": along(4 * d)})
 
     def w_near(i):
         blk = wblk(4 * i, x)
@@ -124,10 +128,10 @@
             send(blk, blk, out_sem.at[0], r_wz.at[4 * i + j], {"z": along(e)})
 
     def w_arrive(r):
-        dev = sender(r % 4) if r % 4 else {"z": along(4 * (r // 4))}
+        dev = sender(r % 4) if r % 4 else {"z": along(-4 * d) if r == 8 else along(4 * (r // 4))}
         got(wblk(r, x), out_sem.at[0], r_wz.at[r], dev)
 
-    groups = ((0,), (1, 2, 3), (4, 12, 8), (5, 6, 7), (13, 14, 15), (9, 10, 11))
+    groups = ((0,), (1, 2, 3), (4,), (12, 8), (13, 14, 15), (9, 10, 11))
 
     def group_of(r):
         return [r in g for g in groups].index(True)
@@ -153,12 +157,16 @@
         return og.at[source(4 * i, d), xi, c]
 
     def o_far():
-        for i, e in ((1, -4), (3, 4), (2, 8)):
+        for i, e in ((1, -4), (3, 4)):
             send(oown, oown, out_sem.at[12], r_oz.at[i], {"z": along(e)})
+
+    def o_farther():
+        blk = og.at[along(-4 * d), x, c]
+        send(blk, blk, out_sem.at[12], r_oz.at[2], {"z": along(4 * d)})
 
     def o_side(i):
         if i:
-            got(oblk(i, x), out_sem.at[12], r_oz.at[i], {"z": along(4 * i)})
+            got(oblk(i, x), out_sem.at[12], r_oz.at[i], {"z": along(-4 * d) if i == 2 else along(4 * i)})
         send(oblk(i, x), oblk(i, x), out_sem.at[3], r_ox.at[i], {"x": xr})
         send(oblk(i, x), oblk(i, x), out_sem.at[3], r_ox.at[4 + i], {"x": xl})
 
@@ -168,7 +176,7 @@
 
     def o_pair(r):
         four = og.at[source(r, d), :, c]
-        send(four, four, out_sem.at[5], r_op.at[0], {"c": other})
+        send(four, four, out_sem.at[5], r_op.at[4 if r % 4 == 3 else r // 4], {"c": other})
 
     def o_near(i):
         got(oblk(i, xr), out_sem.at[3], r_ox.at[4 + i], {"x": xr})
@@ -185,12 +193,12 @@
 
     o_plan = (
         (o_far, lambda: o_side(0)),
-        (lambda: o_side(1), lambda: o_side(3)),
-        (lambda: o_side(2), lambda: o_near(0)),
-        (lambda: o_relay(1), lambda: o_relay(3), lambda: o_relay(2)),
-        (lambda: o_near(1), lambda: o_near(3)),
+        (lambda: o_side(1), lambda: o_side(3), o_farther),
+        (),
+        (lambda: o_relay(1), lambda: o_relay(3)),
+        (lambda: o_relay(2),),
+        (lambda: o_last(0),),
         (lambda: o_near(2),),
-        (lambda: o_last(0),),
         (lambda: o_last(1), lambda: o_last(3)),
         (lambda: o_last(2),),
     )
@@ -202,9 +210,22 @@
     def w_arrivals(*rs):
         for r in rs:
             w_arrive(r)
-            if r % 4 == 0:
+            if r == 12:
+                w_farther()
+            if r in (8, 12):
                 w_near(r // 4)
             w_side(r)
+
+    def w_bundle():
+        four = wg.at[source(4, d), :, c]
+        for j, e in ((1, 1), (2, -1), (3, 2 * d)):
+            send(four, four, out_sem.at[0], r_wz.at[4 + j], {"z": along(e)})
+
+    def w_bundles_in():
+        for r in (5, 6, 7):
+            four = wg.at[source(r, d), :, c]
+            got(four, out_sem.at[0], r_wz.at[r], sender(r % 4))
+            send(four, four, out_sem.at[2], r_wp.at[0], {"c": other})
 
     def w_relays(*rs):
         for r in rs:
@@ -222,44 +243,54 @@
     phase("relB")
     w_relays(0)
     phase("arrC")
-    w_arrivals(4, 12)
+    w_arrive(4)
+    w_arrivals(12)
+    w_side(4)
     o_step(0)
+    phase("relF")
+    w_relays(1, 2, 3, 4)
     phase("arrE")
     w_arrivals(8)
-    phase("relF")
-    w_relays(1, 2, 3)
     o_relay(0)
     phase("arrH")
-    w_arrivals(5, 6, 7, 13, 14, 15)
+    w_arrivals(13, 14, 15)
     phase("tok")
     got(tg.at[ym, 0], out_sem.at[6], r_t.at[0], {"y": ym})
     send(tg.at[ym, 0], tg.at[ym, 0], out_sem.at[6], r_t.at[4], {"y": yp})
     got(tg.at[yp, 1], out_sem.at[6], r_t.at[1], {"y": yp})
     send(tg.at[yp, 1], tg.at[yp, 1], out_sem.at[6], r_t.at[5], {"y": ym})
+    phase("pairK")
+    w_pairs(2)
+    w_bundle()
+    phase("o1")
+    o_step(1)
     phase("relI")
-    w_relays(4, 12, 8)
+    w_relays(12, 8)
     phase("arrK")
     w_arrivals(9, 10, 11)
-    phase("o1")
-    o_step(1)
     phase("pairL")
     w_pairs(0, 1)
     phase("relL")
-    w_relays(5, 6, 7, 13, 14, 15)
+    w_relays(13, 14, 15)
     phase("o2")
-    o_step(2)
+    o_near(0)
     phase("pairM")
-    w_pairs(2)
+    w_pairs(3)
     phase("relM")
     w_relays(9, 10, 11)
-    phase("pairN")
-    w_pairs(3, 4)
     phase("o3")
     o_step(3)
+    phase("pairN")
+    w_pairs(4)
+    phase("bundin")
+    w_bundles_in()
+    phase("o3b")
+    o_side(2)
     phase("pairO")
     w_pairs(5)
     phase("o4")
-    o_step(4)
+    o_near(1)
+    o_near(3)
     phase("waitpair")
     got(wg.at[0:8], out_sem.at[2], r_wp.at[0], {"c": other})
     phase("waittok")
@@ -267,7 +298,7 @@
     got(tg.at[yp, 0], out_sem.at[6], r_t.at[3], {"y": yp})
     got(tg.at[y2, 0], out_sem.at[6], r_t.at[4], {"y": ym})
     got(tg.at[y2, 1], out_sem.at[6], r_t.at[5], {"y": yp})
-    o_left = list(range(5, len(o_plan)))
+    o_left = list(range(4, len(o_plan)))
 
     def o_service(count=1):
         for _ in range(count):
@@ -284,22 +315,22 @@
         wb = wg[8:16, :, :, :, lo:hi].reshape(1024, hi - lo)
         return jnp.dot(ta, wa, preferred_element_type=F32) + jnp.dot(tb, wb, preferred_element_type=F32)
 
-    qkv = project(512, 896)
-    kv_s[REACH : REACH + rows] = qkv[:, 256:].astype(BF16)
-    q_s[...] = (qkv[:, :256] * 0.125).astype(BF16)
-    phase("service1")
-    o_service()
-    phase("projglu")
-    send(kv_s.at[128:256], kv_s.at[640:768], out_sem.at[11], r_h.at[2], at_sp(prv))
-    send(kv_s.at[512:640], kv_s.at[0:128], out_sem.at[11], r_h.at[3], at_sp(nxt))
     glu = (project(0, 256) * jax.nn.sigmoid(project(256, 512))).astype(BF16)
     glu_s[16 : 16 + rows] = glu
     for l in range(2):
         padf[l, 16:528] = glu[:, 128 * l : 128 * l + 128].astype(F32)
+    send(glu_s.at[16:32], glu_s.at[528:544], out_sem.at[7], r_h.at[0], at_sp(prv))
+    send(glu_s.at[512:528], glu_s.at[0:16], out_sem.at[7], r_h.at[1], at_sp(nxt))
+    phase("service1")
+    o_service()
+    phase("projqkv")
+    qkv = project(512, 896)
+    kv_s[REACH : REACH + rows] = qkv[:, 256:].astype(BF16)
+    q_s[...] = (qkv[:, :256] * 0.125).astype(BF16)
+    send(kv_s.at[128:256], kv_s.at[640:768], out_sem.at[11], r_h.at[2], at_sp(prv))
+    send(kv_s.at[512:640], kv_s.at[0:128], out_sem.at[11], r_h.at[3], at_sp(nxt))
     phase("service2")
     o_service()
-    send(glu_s.at[16:32], glu_s.at[528:544], out_sem.at[7], r_h.at[0], at_sp(prv))
-    send(glu_s.at[512:528], glu_s.at[0:16], out_sem.at[7], r_h.at[1], at_sp(nxt))
 
     lane64 = lax.broadcasted_iota(jnp.int32, (64, 128), 1)
 
@@ -380,9 +411,9 @@
     for n in range(3):
         phase(f"attend{n}")
         attend(order[n])
-        phase(f"service{n + 4}")
-        o_service()
-    o_service(len(o_left))
+        if n == 1:
+            phase("service4")
+            o_service()
     phase("waitstat")
     got(st_rx, out_sem.at[8], r_st.at[0], {"y": ym})
     phase("norm")
@@ -398,50 +429,110 @@
 
     norm_rows(y2)
 
-    phase("waitout")
-    got(og.at[0:8], out_sem.at[5], r_op.at[0], {"c": other})
-
-    def out_half(block, half):
+    def zcol(i, j):
+        return lax.rem(z + 16 + 4 * i + (0, -1, 1, 2)[j], 16)
+
+    ups = ([(0, 0), (0, 2)], [(1, 0)], [(3, 0), (3, 2)], [(2, 0)], [(0, 3), (1, 3)])
+    downs = ([(0, 1)], [(1, 1), (1, 2)], [(3, 1)], [(2, 1), (2, 2)], [(2, 3), (3, 3)])
+    u_at, d_at = (0, 2, 3, 5, 6, 8), (0, 1, 3, 4, 6, 8)
+
+    def out_group(block, n):
         f = feat[pl.ds(pl.multiple_of(block * 128, 128), 128), :]
-        return nt_dot(f, og[8 * half : 8 * half + 8].reshape(1024, 512))
-
-    phase("outmm")
-    tx2[0] = out_half(y2, 0).astype(BF16)
-    tx2[1] = out_half(y2, 1).astype(BF16)
-    send(tx2.at[0], rx2.at[0], out_sem.at[9], r_r2.at[0], {"y": yp})
+        w = jnp.concatenate([og[zcol(i, j)].reshape(128, 512) for i, j in ups[n] + downs[n]], axis=0)
+        v = nt_dot(f, w)
+        cut = [v[:, 128 * k : 128 * k + 128] for k in range(len(ups[n]) + len(downs[n]))]
+        return cut[: len(ups[n])], cut[len(ups[n]) :]
+
+    def put(ref, first, blocks):
+        for k, v in enumerate(blocks):
+            ref[first + k] = v.astype(ref.dtype)
+
+    def columns_here(n):
+        if n < 4:
+            got(og.at[0:3, :, 0], out_sem.at[5], r_op.at[(0, 1, 3, 2)[n]], {"c": other})
+        else:
+            got(og.at[0:2], out_sem.at[5], r_op.at[4], {"c": other})
+
+    def send_far(n):
+        us, ds = pl.ds(u_at[n], len(ups[n])), pl.ds(d_at[n], len(downs[n]))
+        send(tx2.at[0, us], rx2.at[0, us], out_sem.at[9], r_r2.at[n], {"y": yp})
+        send(tx2.at[1, ds], rx2.at[1, ds], out_sem.at[9], r_r2.at[5 + n], {"y": ym})
+
+    def far_group(n):
+        phase(f"waitout{n}")
+        columns_here(n)
+        phase(f"far{n}")
+        u, dn = out_group(y2, n)
+        put(tx2.at[0], u_at[n], u)
+        put(tx2.at[1], d_at[n], dn)
+
+    far_group(0)
+    far_group(1)
+    send_far(0)
+    far_group(2)
+    send_far(1)
     norm_rows(yp)
-    send(tx2.at[1], rx2.at[1], out_sem.at[9], r_r2.at[1], {"y": ym})
+    send_far(2)
     norm_rows(ym)
-    txp[0, 1] = out_half(yp, 1).astype(BF16)
-    txp[1, 0] = out_half(ym, 0).astype(BF16)
-    send(txp.at[0, 1], rxp.at[0, 1], out_sem.at[10], r_rp.at[1], {"y": yp})
-    part[0] = out_half(yp, 0)
-    send(txp.at[1, 0], rxp.at[1, 0], out_sem.at[10], r_rp.at[2], {"y": ym})
-    part[1] = out_half(ym, 1)
+    phase("service7")
+    o_service(len(o_left))
+    far_group(3)
+    far_group(4)
+    send_far(3)
+    phase("near")
+    for n in range(5):
+        u, dn = out_group(yp, n)
+        put(part.at[0], u_at[n], u)
+        put(tx4.at[0, 1], d_at[n], dn)
+        if n == 0:
+            send_far(4)
+    for n in range(5):
+        u, dn = out_group(ym, n)
+        put(tx4.at[1, 0], u_at[n], u)
+        put(part.at[1], d_at[n], dn)
+        if n == 0:
+            send(tx4.at[0, 1], rx4.at[0, 1], out_sem.at[10], r_rp.at[0], {"y": yp})
     phase("attendown")
     attend(y)
+    send(tx4.at[1, 0], rx4.at[1, 0], out_sem.at[10], r_rp.at[1], {"y": ym})
     norm_rows(y)
-    part[2] = out_half(y, 0)
-    part[3] = out_half(y, 1)
+    for n in range(5):
+        u, dn = out_group(y, n)
+        put(part.at[2], u_at[n], u)
+        put(part.at[3], d_at[n], dn)
+
+    def send_near(n):
+        us, ds = pl.ds(u_at[n], len(ups[n])), pl.ds(d_at[n], len(downs[n]))
+        send(tx4.at[0, 0, us], rx4.at[0, 0, us], out_sem.at[10], r_rp.at[2], {"y": yp})
+        send(tx4.at[1, 1, ds], rx4.at[1, 1, ds], out_sem.at[10], r_rp.at[3], {"y": ym})
+
     phase("wait2")
-    got(rx2.at[0], out_sem.at[9], r_r2.at[0], {"y": ym})
-    txp[0, 0] = (part[0] + rx2[0].astype(F32)).astype(BF16)
-    got(rx2.at[1], out_sem.at[9], r_r2.at[1], {"y": yp})
-    txp[1, 1] = (part[1] + rx2[1].astype(F32)).astype(BF16)
-    send(txp.at[0, 0], rxp.at[0, 0], out_sem.at[10], r_rp.at[0], {"y": yp})
-    send(txp.at[1, 1], rxp.at[1, 1], out_sem.at[10], r_rp.at[3], {"y": ym})
+    for n in range(5):
+        us, ds = pl.ds(u_at[n], len(ups[n])), pl.ds(d_at[n], len(downs[n]))
+        got(rx2.at[0, us], out_sem.at[9], r_r2.at[n], {"y": ym})
+        tx4[0, 0, us] = (part[0, us] + rx2[0, us].astype(F32)).astype(BF16)
+        got(rx2.at[1, ds], out_sem.at[9], r_r2.at[5 + n], {"y": yp})
+        tx4[1, 1, ds] = (part[1, ds] + rx2[1, ds].astype(F32)).astype(BF16)
+        if n:
+            send_near(n - 1)
     phase("waitfin")
     log_out[...] = jnp.transpose(lstat[...])[0:4, :]
-    for a, h in ((0, 1), (1, 0), (0, 0), (1, 1)):
-        got(rxp.at[a, h], out_sem.at[10], r_rp.at[2 * a + h], {"y": ym if a == 0 else yp})
+    send_near(4)
+    got(rx4.at[0, 1], out_sem.at[10], r_rp.at[0], {"y": ym})
+    got(rx4.at[1, 0], out_sem.at[10], r_rp.at[1], {"y": yp})
+    got(rx4.at[0, 0], out_sem.at[10], r_rp.at[2], {"y": ym})
+    got(rx4.at[1, 1], out_sem.at[10], r_rp.at[3], {"y": yp})
     phase("final")
-    for h in range(2):
-        total = part[2 + h] + rxp[0, h].astype(F32) + rxp[1, h].astype(F32)
-        mixed[:, 1024 * h : 1024 * h + 1024] = total.astype(BF16)
+    for way, at, sets in ((0, u_at, ups), (1, d_at, downs)):
+        for n in range(5):
+            for k, (i, j) in enumerate(sets[n]):
+                p = at[n] + k
+                total = part[2 + way, p] + rx4[0, way, p].astype(F32) + rx4[1, way, p].astype(F32)
+                mixed[:, pl.ds(pl.multiple_of(zcol(i, j) * 128, 128), 128)] = total.astype(BF16)
     phase("drain")
     for i, ref in enumerate((
-        wg.at[0:5, 0:3, 0], wg.at[0:6], wg.at[0:8], og.at[0:3, :, 0], og.at[0:6], og.at[0:8], tg.at[0:3],
-        glu_s.at[0:32], st_rx, tx2, txp, kv_s.at[0:256], og.at[0:3, 0, 0],
+        wg.at[0:3], wg.at[0:13, 0:3, 0], wg.at[0:8], og.at[0:3, :, 0], og.at[0:6], og.at[0:8], tg.at[0:3],
+        glu_s.at[0:32], st_rx, tx2, tx4, kv_s.at[0:256], og.at[0:3, 0, 0],
     )):
         copy(ref, ref, out_sem.at[i], r_wp.at[0], {"c": other}).wait_send()
     phase(None)
@@ -462,6 +553,7 @@
         pltpu.VMEM((1, 256), F32),
         pltpu.VMEM((1, 256), F32),
         pltpu.VMEM((1, 256), F32),
+        pltpu.SMEM((4,), F32),
         pltpu.VMEM((16, 4, 2, 16, 896), BF16),
         pltpu.VMEM((16, 4, 2, 16, 512), BF16),
         pltpu.VMEM((4, 2, 128, 1024), BF16),
@@ -477,14 +569,14 @@
         pltpu.VMEM((3, 8, 512), F32),
         pltpu.VMEM((512, 512), BF16),
         pltpu.VMEM((128, 384), F32),
-        pltpu.VMEM((4, 128, 1024), F32),
-        pltpu.VMEM((2, 128, 1024), BF16),
-        pltpu.VMEM((2, 128, 1024), BF16),
-        pltpu.VMEM((2, 2, 128, 1024), BF16),
-        pltpu.VMEM((2, 2, 128, 1024), BF16),
-        dma((13,)),
+        pltpu.VMEM((4, 8, 128, 128), F32),
+        pltpu.VMEM((2, 8, 128, 128), BF16),
+        pltpu.VMEM((2, 8, 128, 128), BF16),
+        pltpu.VMEM((2, 2, 8, 128, 128), BF16),
+        pltpu.VMEM((2, 2, 8, 128, 128), BF16),
+        dma((14,)),
     ]
-    for n in (16, 16, 12, 1, 12, 4, 4, 1, 6, 4, 1, 2, 4, 13):
+    for n in (16, 16, 12, 1, 12, 4, 4, 5, 6, 4, 1, 10, 4, 13):
         scratch += [dma((n,))]
     mixed, log_total = pl.pallas_call(
         layer,
@@ -493,7 +585,7 @@
             pltpu.VMEM((128, 2048), BF16),
             pltpu.VMEM((4, 512), F32),
         ),
-        in_specs=[pl.BlockSpec(memory_space=pl.ANY)] * 13 + [pl.BlockSpec(memory_space=pltpu.SMEM)],
+        in_specs=[pl.BlockSpec(memory_space=pl.ANY)] * 14,
         out_specs=(vm, vm),
         scratch_shapes=scratch,
         compiler_params=pltpu.CompilerParams(

time: 78.6 us -> 71.7 us (0.912); the launches traced: 77.6 us -> 71.5 us
  Pallas kernels: 75.6 us -> 69.5 us
    pallas_call x1, Pallas kernels: 75.6 us -> 69.5 us  [on_device(): pl.pallas_call(layer, name='layer', out_shape=(pltpu.VMEM((128, 2048), BF...]
where the time goes in v3:
time: 71.7 us; the launch traced here: 71.5 us
  Pallas kernels  69.5 us (97%)
  local copies, waits for them, and re-layouts  1.39 us (2%)
    pallas_call x1, Pallas kernels, on_device(): pl.pallas_call(layer, name='layer', out_shape=(pltpu.VMEM((128, 2048), BF...  69.5 us

profile of v3, /device:TPU:1, one launch (start us, length us, event | category | flops | bytes accessed | tf_op | source)
XLA Modules:
  0.0 71.5 jit_solution(16501068964770057457)
XLA Ops:
  0.6 69.5 %layer.1 = (bf16[128,2048]{1,0:T(8,128)(2,1)S(1)}, f32[4,512]{1,0:T(4,128)S(1)}) custom-call(bf16[128,2048]{1,0:T(8,128)(2,1)} %tok_h.1, f32[1,2048]{1,0:T(1,128)} %bitcast.8, bf16[16,256]{1,0:T(8,128)(2,1)} %val_h.1, bf16[16,256]{1,0:T(8,128)(2,1)} %gate_h.1, bf16[16,256]{1,0:T(8,128)(2,1)} %wq_h.1, bf16[16,64]{1,0:T(8,128)(2,1)} %wk_h.1, ...), custom_call_target="tpu_custom_call" | custom-call | tf_op jit(solution)/shard_map/layer/pallas_call | solution.py:581
  70.1 0.8 %copy.18 = bf16[128,2048]{1,0:T(8,128)(2,1)} copy(bf16[128,2048]{1,0:T(8,128)(2,1)S(1)} %get-tuple-element.6) | data formatting | bytes 1048576
  70.9 0.6 copy.19

commit v4 on v3

--- a/solution.py
+++ b/solution.py
@@ -130,6 +130,17 @@
     def w_arrive(r):
         dev = sender(r % 4) if r % 4 else {"z": along(-4 * d) if r == 8 else along(4 * (r // 4))}
         got(wblk(r, x), out_sem.at[0], r_wz.at[r], dev)
+
+    def w_last_early():
+        got(wg.at[0, 0:3, 0], out_sem.at[1], r_wg.at[5], {"x": xr})
+        for r in groups[5]:
+            for xi in (x, xl, xr):
+                send(wblk(r, xi), wblk(r, xi), out_sem.at[2], r_wp.at[0], {"c": other})
+
+    def w_last():
+        got(wg.at[0, 0:3, 0], out_sem.at[1], r_wg.at[11], {"x": xl})
+        for r in groups[5]:
+            send(wblk(r, x2), wblk(r, x2), out_sem.at[2], r_wp.at[0], {"c": other})
 
     groups = ((0,), (1, 2, 3), (4,), (12, 8), (13, 14, 15), (9, 10, 11))
 
@@ -284,10 +295,12 @@
     w_pairs(4)
     phase("bundin")
     w_bundles_in()
+    phase("pairO")
+    w_last_early()
     phase("o3b")
     o_side(2)
-    phase("pairO")
-    w_pairs(5)
+    phase("pairP")
+    w_last()
     phase("o4")
     o_near(1)
     o_near(3)
@@ -367,21 +380,28 @@
     conv_rows(7, 0)
     st_tx[...] = jnp.transpose(stat[...])[0:8, :]
 
+    phase("kvprep")
+    low = lax.broadcasted_iota(jnp.int32, (512, 128), 1) < 64
+
+    def widen(r0, n):
+        kvf = kv_s[r0 : r0 + n].astype(F32)
+        turned = pltpu.roll(kvf, 64, 1)
+        lo = low[:n]
+        kvw[0, r0 : r0 + n] = jnp.where(lo, kvf, 0.0).astype(BF16)
+        kvw[1, r0 : r0 + n] = jnp.where(lo, 0.0, turned).astype(BF16)
+        kvw[2, r0 : r0 + n] = jnp.where(lo, turned, 0.0).astype(BF16)
+        kvw[3, r0 : r0 + n] = jnp.where(lo, 0.0, kvf).astype(BF16)
+
+    widen(128, 512)
+    for i, dev in enumerate((yp, ym, y2)):
+        send(st_tx, st_rx.at[i], out_sem.at[8], r_st.at[0], {"y": dev})
     phase("waitkv")
     got(kv_s.at[640:768], out_sem.at[11], r_h.at[2], at_sp(nxt))
     got(kv_s.at[0:128], out_sem.at[11], r_h.at[3], at_sp(prv))
-    for i, dev in enumerate((yp, ym, y2)):
-        send(st_tx, st_rx.at[i], out_sem.at[8], r_st.at[0], {"y": dev})
-    phase("kvprep")
-    kvf = kv_s[...].astype(F32)
-    turned = pltpu.roll(kvf, 64, 1)
-    low = lax.broadcasted_iota(jnp.int32, (768, 128), 1) < 64
-    kvw[0] = jnp.where(low, kvf, 0.0).astype(BF16)
-    kvw[1] = jnp.where(low, 0.0, turned).astype(BF16)
-    kvw[2] = jnp.where(low, turned, 0.0).astype(BF16)
-    kvw[3] = jnp.where(low, 0.0, kvf).astype(BF16)
-
-    phase("attend")
+    phase("kvprep2")
+    widen(0, 128)
+    widen(640, 128)
+
     low128 = lax.broadcasted_iota(jnp.int32, (128, 128), 1) < 64
     ends = lax.broadcasted_iota(jnp.int32, (1, 384), 1)
 

time: 71.7 us -> 71 us (level)
  no operation moved by 1% of the time
where the time goes in v4:
time: 71 us; the launch traced here: 70.8 us
  Pallas kernels  68.8 us (97%)
  local copies, waits for them, and re-layouts  1.39 us (2%)
    pallas_call x1, Pallas kernels, on_device(): pl.pallas_call(layer, name='layer', out_shape=(pltpu.VMEM((128, 2048), BF...  68.8 us

profile of v4, /device:TPU:1, one launch (start us, length us, event | category | flops | bytes accessed | tf_op | source)
XLA Modules:
  0.0 70.8 jit_solution(15685330878701329812)
XLA Ops:
  0.6 68.8 %layer.1 = (bf16[128,2048]{1,0:T(8,128)(2,1)S(1)}, f32[4,512]{1,0:T(4,128)S(1)}) custom-call(bf16[128,2048]{1,0:T(8,128)(2,1)} %tok_h.1, f32[1,2048]{1,0:T(1,128)} %bitcast.8, bf16[16,256]{1,0:T(8,128)(2,1)} %val_h.1, bf16[16,256]{1,0:T(8,128)(2,1)} %gate_h.1, bf16[16,256]{1,0:T(8,128)(2,1)} %wq_h.1, bf16[16,64]{1,0:T(8,128)(2,1)} %wk_h.1, ...), custom_call_target="tpu_custom_call" | custom-call | tf_op jit(solution)/shard_map/layer/pallas_call | solution.py:601
  69.5 0.8 %copy.18 = bf16[128,2048]{1,0:T(8,128)(2,1)} copy(bf16[128,2048]{1,0:T(8,128)(2,1)S(1)} %get-tuple-element.6) | data formatting | bytes 1048576
  70.2 0.6 copy.19

commit v5 on v4

--- a/solution.py
+++ b/solution.py
@@ -437,13 +437,13 @@
     phase("waitstat")
     got(st_rx, out_sem.at[8], r_st.at[0], {"y": ym})
     phase("norm")
-    both = st_tx[...] + st_rx[0] + st_rx[1] + st_rx[2]
-    stat[...] = jnp.transpose(jnp.concatenate([both, jnp.zeros((120, 512), F32)], axis=0)) * (1.0 / 1024.0)
+    st_rx[0] = (st_tx[...] + st_rx[0] + st_rx[1] + st_rx[2]) * (1.0 / 1024.0)
 
     def norm_rows(i):
         r0 = pl.multiple_of(i * 128, 128)
-        mean = stat[pl.ds(r0, 128), 0:1]
-        var = stat[pl.ds(r0, 128), 1:2] - mean * mean
+        both = jnp.transpose(jnp.concatenate([st_rx[0, :, pl.ds(r0, 128)], jnp.zeros((120, 128), F32)], axis=0))
+        mean = both[:, 0:1]
+        var = both[:, 1:2] - mean * mean
         v = (filt[pl.ds(r0, 128), :] - mean) * lax.rsqrt(var + 1e-05) * ngain[...] + nbias[...]
         feat[pl.ds(r0, 128), 0:256] = (v * jax.nn.sigmoid(v)).astype(BF16)
 

time: 71 us -> 71.1 us (level)
  no operation moved by 1% of the time
where the time goes in v5:
time: 71.1 us; the launch traced here: 70.9 us
  Pallas kernels  68.9 us (97%)
  local copies, waits for them, and re-layouts  1.39 us (2%)
    pallas_call x1, Pallas kernels, on_device(): pl.pallas_call(layer, name='layer', out_shape=(pltpu.VMEM((128, 2048), BF...  68.9 us

profile of v5, /device:TPU:1, one launch (start us, length us, event | category | flops | bytes accessed | tf_op | source)
XLA Modules:
  0.0 70.9 jit_solution(4163878514498486335)
XLA Ops:
  0.6 68.9 %layer.1 = (bf16[128,2048]{1,0:T(8,128)(2,1)S(1)}, f32[4,512]{1,0:T(4,128)S(1)}) custom-call(bf16[128,2048]{1,0:T(8,128)(2,1)} %tok_h.1, f32[1,2048]{1,0:T(1,128)} %bitcast.8, bf16[16,256]{1,0:T(8,128)(2,1)} %val_h.1, bf16[16,256]{1,0:T(8,128)(2,1)} %gate_h.1, bf16[16,256]{1,0:T(8,128)(2,1)} %wq_h.1, bf16[16,64]{1,0:T(8,128)(2,1)} %wk_h.1, ...), custom_call_target="tpu_custom_call" | custom-call | tf_op jit(solution)/shard_map/layer/pallas_call | solution.py:601
  69.5 0.8 %copy.18 = bf16[128,2048]{1,0:T(8,128)(2,1)} copy(bf16[128,2048]{1,0:T(8,128)(2,1)S(1)} %get-tuple-element.6) | data formatting | bytes 1048576
  70.3 0.6 copy.19
